TPU v7x, 32 devices: a whole 2x2x4 slice. The times are simulated.
32 devices in a mesh: fs: 16 (over z, y, x), tp: 2 (over core).
Axes of the slice: x: 2, y: 2, z: 4, core: 2. Of those that a mesh axis runs over, the one named last changes fastest.
Arguments:
- tokens: bfloat16 [6144, 2048], P('fs'), may hold values from -6 to 6
- merged: bfloat16 [6144, 2048], P('fs'), may hold values from -6 to 6
- gain_first: float32 [2048], replicated, may hold values from 0.1 to 1.9
- gate_first: bfloat16 [2048, 2816], P('fs', 'tp'), may hold values from -0.125 to 0.125
- up_first: bfloat16 [2048, 2816], P('fs', 'tp'), may hold values from -0.125 to 0.125
- down_first: bfloat16 [2816, 2048], P('tp', 'fs'), may hold values from -0.21875 to 0.21875
- gain_second: float32 [2048], replicated, may hold values from 0.1 to 1.9
- gate_second: bfloat16 [2048, 2816], P('fs', 'tp'), may hold values from -0.125 to 0.125
- up_second: bfloat16 [2048, 2816], P('fs', 'tp'), may hold values from -0.125 to 0.125
- down_second: bfloat16 [2816, 2048], P('tp', 'fs'), may hold values from -0.21875 to 0.21875
Outputs:
- result: bfloat16 [6144, 2048], P('fs')
All inputs are finite; a program needn't handle non-finite values.
Results may differ from a plain program's by a relative error of at most 0.01.
Values may be sent and summed in bfloat16 or wider, within the bound.
A program may use at most 64 MiB of HBM per device.

v0:
```python
import functools

import jax
import jax.numpy as jnp
from jax import lax
from jax.experimental import pallas as pl
from jax.experimental.pallas import tpu as pltpu
from jax.sharding import PartitionSpec as P

EPS = 1e-06
BF16 = jnp.bfloat16
F32 = jnp.float32
PLANE = 4
RING = 4


def norm_rows(values, gain):
    scale = lax.rsqrt(jnp.mean(values * values, axis=-1, keepdims=True) + EPS)
    return values * scale * gain


def gathered_block(normed, gate, up, down):
    gate_whole = lax.all_gather(gate, "fs", axis=0, tiled=True)
    up_whole = lax.all_gather(up, "fs", axis=0, tiled=True)
    g = jnp.dot(normed, gate_whole, preferred_element_type=F32)
    u = jnp.dot(normed, up_whole, preferred_element_type=F32)
    hidden = (jax.nn.silu(g) * u).astype(BF16)
    down_whole = lax.all_gather(down, "fs", axis=1, tiled=True)
    part = jnp.dot(hidden, down_whole, preferred_element_type=F32)
    return lax.psum(part.astype(BF16), "tp").astype(F32)


def gathered_shards(tokens, merged, gain1, g1, u1, d1, gain2, g2, u2, d2):
    source = tokens.astype(F32)
    middle = source + merged.astype(F32)
    normed = norm_rows(source, gain1).astype(BF16)
    middle = middle + 0.5 * gathered_block(normed, g1, u1, d1)
    normed = norm_rows(middle, gain2).astype(BF16)
    return (middle + 0.5 * gathered_block(normed, g2, u2, d2)).astype(BF16)


def kernel(
    tokens, merged, gain1, gain2, wa, wb, wc, wd, we, wf, out,
    w, normed1, normed2, hidden, part, own, sib, comb, diag, rsr, middle, fin,
    p1_s, p1_r, p1_l, ring_s, ring_r, fwd_s, fwd_r,
    ag_s, ag_r, rel_s, rel_r, sib_s, sib_r, rs_s, rs_r, fin_s, fin_r,
):
    shards_in = (wa, wb, wc, wd, we, wf)
    fs = lax.axis_index("fs")
    t = lax.axis_index("tp")
    z = fs // PLANE
    p = fs % PLANE
    rows, width = tokens.shape
    half = rows // 2
    quarter = half // 2
    q, pw = w.shape[1], width // RING
    ds = wa.shape[1]
    qh = q // 2

    def dev(zz, pp, tt):
        return {"fs": zz * PLANE + pp, "tp": tt}

    peers = (p, p + 1 - 2 * (p % 2), (p + 2) % PLANE, PLANE - 1 - p)

    zc, zb, zo = (z + 1) % RING, (z + RING - 1) % RING, (z + 2) % RING
    cw, ccw, sibling = dev(zc, p, t), dev(zb, p, t), dev(z, p, 1 - t)
    to_peer = [dev(z, pp, t) for pp in peers]

    def remote(src, dst, s, r, to):
        return pltpu.make_async_remote_copy(
            src_ref=src, dst_ref=dst, send_sem=s, recv_sem=r,
            device_id=to, device_id_type=pl.DeviceIdType.MESH,
        )

    mine = pl.ds(pl.multiple_of(t * half, 16), half)
    other = pl.ds(pl.multiple_of((1 - t) * half, 16), half)

    barrier = pltpu.get_barrier_semaphore()
    targets = [cw, ccw, sibling] + to_peer[1:]
    for to in targets:
        pl.semaphore_signal(barrier, inc=1, device_id=to, device_id_type=pl.DeviceIdType.MESH)
    pl.semaphore_wait(barrier, len(targets))

    def p1_lanes(pp):
        return pl.ds(pl.multiple_of((z * PLANE + pp) * ds, ds), ds)

    def p1(m, r):
        src = shards_in[m].at[pl.ds(pl.multiple_of(peers[r] * q, 16), q), :]
        return remote(src, w.at[m, :, p1_lanes(p)], p1_s.at[m, r - 1], p1_r.at[m, r - 1], to_peer[r])

    def p1_local(m):
        src = shards_in[m].at[pl.ds(pl.multiple_of(p * q, 16), q), :]
        return pltpu.make_async_copy(src, w.at[m, :, p1_lanes(p)], p1_l.at[m])

    def p1_in(m, r):
        src = w.at[m, :, p1_lanes(peers[r])]
        return remote(src, src, p1_s.at[m, r - 1], p1_r.at[m, r - 1], to_peer[r])

    def start_p1(m):
        for r in (3, 1, 2):
            p1(m, r).start()
        p1_local(m).start()

    def blk(m, zz, lo=0, n=None):
        return w.at[m, pl.ds(lo, q if n is None else n), pl.ds(pl.multiple_of(zz * pw, pw), pw)]

    def ring(m, k, zz):
        return remote(blk(m, zz), blk(m, zz), ring_s.at[m, k], ring_r.at[m, k], (cw, ccw)[k])

    def fwd(m, k, zz):
        return remote(blk(m, zz, k * qh, qh), blk(m, zz, k * qh, qh), fwd_s.at[m, k], fwd_r.at[m, k], (cw, ccw)[k])

    def own_ring(m):
        p1_local(m).wait()
        for r in (1, 2, 3):
            p1_in(m, r).wait_recv()
        ring(m, 0, z).start()
        ring(m, 1, z).start()

    def service(m):
        ring(m, 0, zb).wait_recv()
        fwd(m, 0, zb).start()
        ring(m, 1, zc).wait_recv()
        fwd(m, 1, zc).start()

    def arrived(m):
        fwd(m, 0, zo).wait_recv()
        fwd(m, 1, zo).wait_recv()

    bufs = (normed1, normed2)

    def piece(tt, h):
        return pl.ds(pl.multiple_of(tt * half + h * quarter, 16), quarter)

    def ag(f, r, h):
        at = piece(t, h)
        return remote(bufs[f].at[0, at, :], bufs[f].at[r, at, :], ag_s.at[f, r - 1, h], ag_r.at[f, r - 1, h], to_peer[r])

    def ag_on(f, h):
        at = piece(t, h)
        return remote(bufs[f].at[2 - h, at, :], bufs[f].at[3, at, :], ag_s.at[f, 2, h], ag_r.at[f, 2, h], to_peer[1 + h])

    def relay(f, r, h, tt):
        at = bufs[f].at[r, piece(tt, h), :]
        return remote(at, at, rel_s.at[f, r, h], rel_r.at[f, r, h], sibling)

    def ag_near(f):
        for r, h in ((2, 0), (1, 1)):
            ag(f, r, h).wait_recv()
            ag_on(f, h).start()
            relay(f, r, h, t).start()
        for r, h in ((2, 1), (1, 0)):
            ag(f, r, h).wait_recv()
            relay(f, r, h, t).start()

    def ag_far(f):
        for h in range(2):
            ag_on(f, h).wait_recv()
            relay(f, 3, h, t).start()

    def relayed(f, r):
        for h in range(2):
            relay(f, r, h, 1 - t).wait_recv()

    lanes = [pl.ds(pl.multiple_of(zz * pw, pw), pw) for zz in (z, zb, zc, zo)]
    first, second = pl.ds(0, quarter), pl.ds(quarter, quarter)

    def to_sibling(f, c, r):
        return remote(part.at[r, :, lanes[c]], sib.at[r, :, lanes[c]], sib_s.at[f, c, r], sib_r.at[f, c, r], sibling)

    def rs(f, c, kind):
        at = lanes[c]
        src, dst, r = (
            (comb.at[2, first, at], diag.at[0, :, at], 1),
            (comb.at[2, second, at], diag.at[1, :, at], 2),
            (comb.at[0, first, at], rsr.at[0, first, at], 1),
            (comb.at[0, second, at], rsr.at[0, second, at], 1),
            (comb.at[1, second, at], rsr.at[1, second, at], 2),
            (comb.at[1, first, at], rsr.at[1, first, at], 2),
        )[kind]
        return remote(src, dst, rs_s.at[f, c, kind], rs_r.at[f, c, kind], to_peer[r])

    def make_hidden(f, slot):
        @pl.loop(0, 2)
        def _(i):
            at = pl.ds(pl.multiple_of(i * half, 16), half)
            x = bufs[f][slot, at, :]
            dims = (((1,), (1,)), ((), ()))
            g = lax.dot_general(x, w[3 * f], dims, preferred_element_type=F32)
            u = lax.dot_general(x, w[3 * f + 1], dims, preferred_element_type=F32)
            hidden[slot, at, :] = (g / (1.0 + jnp.exp(-g)) * u).astype(BF16)

    def make_down(f, c):
        at = lanes[c]

        @pl.loop(0, PLANE)
        def _(k):
            r = PLANE - 1 - k
            part[r, :, at] = jnp.dot(hidden[r, other, :], w[3 * f + 2, :, at], preferred_element_type=F32).astype(BF16)
            to_sibling(f, c, r).start()
            own[r, :, at] = jnp.dot(hidden[r, mine, :], w[3 * f + 2, :, at], preferred_element_type=F32).astype(BF16)

    step = 16

    def down(f, c):
        at = lanes[c]
        make_down(f, c)
        for r, kinds in ((3, (0, 1)), (1, (2,)), (2, (4,))):
            to_sibling(f, c, r).wait_recv()

            @pl.loop(0, half // (2 * step))
            def _(i):
                some = pl.ds(pl.multiple_of(i * 2 * step, step), 2 * step)
                comb[r - 1, some, at] = (own[r, some, at].astype(F32) + sib[r, some, at].astype(F32)).astype(BF16)

            for kind in kinds:
                rs(f, c, kind).start()
        to_sibling(f, c, 0).wait_recv()

    def finish(f, c):
        at = lanes[c]
        rs(f, c, 0).wait_recv()
        comb[1, first, at] = (comb[1, first, at].astype(F32) + diag[0, :, at].astype(F32)).astype(BF16)
        rs(f, c, 5).start()
        rs(f, c, 1).wait_recv()
        comb[0, second, at] = (comb[0, second, at].astype(F32) + diag[1, :, at].astype(F32)).astype(BF16)
        rs(f, c, 3).start()

    def all_down(f, before_last):
        down(f, 0)
        service(3 * f + 2)
        before_last()
        down(f, 1)
        finish(f, 0)
        down(f, 2)
        finish(f, 1)
        arrived(3 * f + 2)
        down(f, 3)
        finish(f, 2)
        finish(f, 3)

    def landed(f):
        for c in range(RING):
            for kind in (2, 3, 4, 5):
                rs(f, c, kind).wait_recv()

    def reduced(at):
        total = own[0, at, :].astype(F32) + sib[0, at, :].astype(F32)
        return total + rsr[0, at, :].astype(F32) + rsr[1, at, :].astype(F32)

    start_p1(0)
    start_p1(1)
    start_p1(2)

    @pl.loop(0, rows // step)
    def _(i):
        at = pl.ds(pl.multiple_of(i * step, step), step)
        normed1[0, at, :] = norm_rows(tokens[at, :].astype(F32), gain1[...]).astype(BF16)

    for r, h in ((2, 0), (1, 1), (2, 1), (1, 0)):
        ag(0, r, h).start()
    for m in (3, 4, 5):
        start_p1(m)
    own_ring(0)
    own_ring(1)
    service(0)
    own_ring(2)
    ag_near(0)
    service(1)
    own_ring(3)
    ag_far(0)
    arrived(0)
    arrived(1)
    for r in range(PLANE):
        if r:
            relayed(0, r)
        make_hidden(0, r)
    all_down(0, lambda: own_ring(4))
    service(3)
    own_ring(5)
    landed(0)
    for h in range(2):

        @pl.loop(0, quarter // step)
        def _(i):
            at = pl.ds(pl.multiple_of(h * quarter + i * step, step), step)
            full = pl.ds(pl.multiple_of(t * half + h * quarter + i * step, step), step)
            value = tokens[full, :].astype(F32) + merged[full, :].astype(F32) + 0.5 * reduced(at)
            middle[at, :] = value
            normed2[0, full, :] = norm_rows(value, gain2[...]).astype(BF16)

        for r in (2 - h, 1 + h):
            ag(1, r, h).start()
        relay(1, 0, h, t).start()

    ag_near(1)
    service(4)
    ag_far(1)
    arrived(3)
    arrived(4)
    for r in range(PLANE):
        relayed(1, r)
        make_hidden(1, r)
    for c in range(RING):
        for r in range(PLANE):
            to_sibling(0, c, r).wait_send()
        for kind in range(6):
            rs(0, c, kind).wait_send()
    all_down(1, lambda: None)
    landed(1)

    @pl.loop(0, half // step)
    def _(i):
        at = pl.ds(pl.multiple_of(i * step, step), step)
        full = pl.ds(pl.multiple_of(t * half + i * step, step), step)
        out[full, :] = (middle[at, :] + 0.5 * reduced(at)).astype(BF16)

    last = remote(out.at[mine, :], fin, fin_s, fin_r, sibling)
    last.start()
    for m in range(6):
        for r in (1, 2, 3):
            p1(m, r).wait_send()
        for k in range(2):
            ring(m, k, z).wait_send()
            fwd(m, k, (zb, zc)[k]).wait_send()
    for f in range(2):
        for h in range(2):
            for r in (1, 2):
                ag(f, r, h).wait_send()
            ag_on(f, h).wait_send()
            for r in range(1 - f, PLANE):
                relay(f, r, h, t).wait_send()
    for c in range(RING):
        for r in range(PLANE):
            to_sibling(1, c, r).wait_send()
        for kind in range(6):
            rs(1, c, kind).wait_send()
    last.wait_recv()
    out[other, :] = fin[...]
    last.wait_send()


def plane_shards(tokens, merged, gain1, g1, u1, d1, gain2, g2, u2, d2):
    rows, width = tokens.shape
    half = rows // 2
    q = d1.shape[0] // PLANE
    vmem = pl.BlockSpec(memory_space=pltpu.VMEM)
    dma = lambda *s: pltpu.SemaphoreType.DMA(s)
    return pl.pallas_call(
        kernel,
        out_shape=jax.ShapeDtypeStruct((rows, width), BF16),
        in_specs=[vmem] * 10,
        out_specs=vmem,
        scratch_shapes=[
            pltpu.VMEM((6, q, width), BF16),
            pltpu.VMEM((PLANE, rows, width), BF16),
            pltpu.VMEM((PLANE, rows, width), BF16),
            pltpu.VMEM((PLANE, rows, q), BF16),
            pltpu.VMEM((PLANE, half, width), BF16),
            pltpu.VMEM((PLANE, half, width), BF16),
            pltpu.VMEM((PLANE, half, width), BF16),
            pltpu.VMEM((PLANE - 1, half, width), BF16),
            pltpu.VMEM((2, half // 2, width), BF16),
            pltpu.VMEM((2, half, width), BF16),
            pltpu.VMEM((half, width), F32),
            pltpu.VMEM((half, width), BF16),
            dma(6, 3), dma(6, 3), dma(6),
            dma(6, 2), dma(6, 2), dma(6, 2), dma(6, 2),
            dma(2, 3, 2), dma(2, 3, 2), dma(2, 4, 2), dma(2, 4, 2),
            dma(2, RING, 4), dma(2, RING, 4), dma(2, RING, 6), dma(2, RING, 6),
            pltpu.SemaphoreType.DMA, pltpu.SemaphoreType.DMA,
        ],
        compiler_params=pltpu.CompilerParams(
            collective_id=0, has_side_effects=True, vmem_limit_bytes=60 * 2**20
        ),
    )(tokens, merged, gain1[None], gain2[None], g1.T, u1.T, d1, g2.T, u2.T, d2)


def shards(n_fs, n_tp, *args):
    rows, width = args[0].shape
    hid, cols = args[5].shape
    fits = n_fs == PLANE * RING and n_tp == 2 and cols % 128 == 0
    fits = fits and hid % (32 * PLANE) == 0 and rows % 64 == 0
    return plane_shards(*args) if fits else gathered_shards(*args)


def solution(mesh):
    return jax.shard_map(
        functools.partial(shards, mesh.shape["fs"], mesh.shape["tp"]),
        mesh=mesh,
        in_specs=(
            P("fs", None),
            P("fs", None),
            P(),
            P("fs", "tp"),
            P("fs", "tp"),
            P("tp", "fs"),
            P(),
            P("fs", "tp"),
            P("fs", "tp"),
            P("tp", "fs"),
        ),
        out_specs=P("fs", None),
        check_vma=False,
    )
```

profile of v0, /device:TPU:0, one launch (start us, length us, event | category | flops | bytes accessed | tf_op | source)
XLA Modules:
  0.0 202.1 jit_solution(6513895156052450390)
XLA Ops:
  0.0 0.0 copy-start.1
  0.0 0.0 copy-start
  0.0 2.0 copy.11
  2.0 1.9 copy.12
  3.8 0.0 copy-done
  3.9 0.9 copy.13
  4.8 0.0 copy-done.1
  4.8 0.9 copy.14
  5.7 193.6 %shard_map.100 = bf16[384,2048]{1,0:T(8,128)(2,1)} custom-call(bf16[384,2048]{1,0:T(8,128)(2,1)} %tokens.1, bf16[384,2048]{1,0:T(8,128)(2,1)} %merged.1, f32[1,2048]{1,0:T(1,128)} %bitcast.10, f32[1,2048]{1,0:T(1,128)} %bitcast.11, bf16[1408,128]{1,0:T(8,128)(2,1)} %bitcast.6, bf16[1408,128]{1,0:T(8,128)(2,1)} %bitcast.7, bf16[1408,128]{1,0:T(8,128)(2,1)} %wc.1, ...), custom_call_target="tpu_custom_call" | custom-call | tf_op jit(solution)/shard_map/pallas_call | solution.py:349
  199.3 2.7 %copy.16 = bf16[384,2048]{1,0:T(8,128)(2,1)} copy(bf16[384,2048]{1,0:T(8,128)(2,1)} %shard_map.100) | data formatting | bytes 3145728
Async XLA Ops:
  0.0 4.8 %copy-start.1 = (bf16[128,1408]{1,0:T(8,128)(2,1)S(1)}, bf16[128,1408]{1,0:T(8,128)(2,1)}, u32[]{:S(2)}) copy-start(bf16[128,1408]{1,0:T(8,128)(2,1)} %param.18) | copy-start | bytes 1081348
  0.0 3.8 %copy-start = (bf16[128,1408]{1,0:T(8,128)(2,1)S(1)}, bf16[128,1408]{1,0:T(8,128)(2,1)}, u32[]{:S(2)}) copy-start(bf16[128,1408]{1,0:T(8,128)(2,1)} %param.17) | copy-start | bytes 1081348
where the time goes:
time: 202 us
  Pallas kernels  194 us (96%)
  local copies, waits for them, and re-layouts  8.42 us (4%)
    pallas_call x1, Pallas kernels, plane_shards(): pl.pallas_call(kernel, out_shape=jax.ShapeDtypeStruct((rows, width), BF16...  194 us
    unnamed x9, local copies, waits for them, and re-layouts  8.42 us

commit v1 on v0

v1 whole, which is shorter than its diff:
```python
import functools

import jax
import jax.numpy as jnp
from jax import lax
from jax.experimental import pallas as pl
from jax.experimental.pallas import tpu as pltpu
from jax.sharding import PartitionSpec as P

EPS = 1e-06
BF16 = jnp.bfloat16
F32 = jnp.float32
PLANE = 4
LINE = 4


def norm_rows(values, gain):
    scale = lax.rsqrt(jnp.mean(values * values, axis=-1, keepdims=True) + EPS)
    return values * scale * gain


def gathered_block(normed, gate, up, down):
    gate_whole = lax.all_gather(gate, "fs", axis=0, tiled=True)
    up_whole = lax.all_gather(up, "fs", axis=0, tiled=True)
    g = jnp.dot(normed, gate_whole, preferred_element_type=F32)
    u = jnp.dot(normed, up_whole, preferred_element_type=F32)
    hidden = (jax.nn.silu(g) * u).astype(BF16)
    down_whole = lax.all_gather(down, "fs", axis=1, tiled=True)
    part = jnp.dot(hidden, down_whole, preferred_element_type=F32)
    return lax.psum(part.astype(BF16), "tp").astype(F32)


def gathered_shards(tokens, merged, gain1, g1, u1, d1, gain2, g2, u2, d2):
    source = tokens.astype(F32)
    middle = source + merged.astype(F32)
    normed = norm_rows(source, gain1).astype(BF16)
    middle = middle + 0.5 * gathered_block(normed, g1, u1, d1)
    normed = norm_rows(middle, gain2).astype(BF16)
    return (middle + 0.5 * gathered_block(normed, g2, u2, d2)).astype(BF16)


def kernel(
    tokens_h, merged_h, gain1, gain2, wa, wb, wc, wd, we, wf, out_h,
    raw, turned, straight, tokens, merged, out, w, normed1, normed2, acc_g, acc_u, hidden,
    part, own, sib, comb, diag, rsr, middle, ssq,
    load, p1_s, p1_r, z_s, z_r,
    ag_s, ag_r, rel_s, rel_r, sib_s, sib_r, rs_s, rs_r, fin_s, fin_r, store,
):
    weights_in = (wa, wb, wc, wd, we, wf)
    fs = lax.axis_index("fs")
    t = lax.axis_index("tp")
    z = fs // PLANE
    p = fs % PLANE
    rows, width = tokens.shape
    half = rows // 2
    quarter = half // 2
    q, pw = w.shape[1], width // LINE
    ds = wc.shape[1]
    step = 16

    def dev(zz, pp, tt):
        return {"fs": zz * PLANE + pp, "tp": tt}

    peers = (p, p + 1 - 2 * (p % 2), (p + 2) % PLANE, PLANE - 1 - p)
    to_peer = [dev(z, pp, t) for pp in peers]
    sibling = dev(z, p, 1 - t)

    low = (z < 2).astype(jnp.int32)
    toward = 2 * low - 1
    mid = (z % 3 != 0).astype(jnp.int32)
    zi, zo = z + toward, z - toward * mid
    inner, outer = dev(zi, p, t), dev(zo, p, t)

    def on_mid(f):
        pl.when(mid == 1)(f)

    def on_end(f):
        pl.when(mid == 0)(f)

    def remote(src, dst, s, r, to):
        return pltpu.make_async_remote_copy(
            src_ref=src, dst_ref=dst, send_sem=s, recv_sem=r,
            device_id=to, device_id_type=pl.DeviceIdType.MESH,
        )

    mine = pl.ds(pl.multiple_of(t * half, 16), half)
    other = pl.ds(pl.multiple_of((1 - t) * half, 16), half)

    def shard_of(m):
        k = m // 3
        return straight.at[k] if m % 3 == 2 else turned.at[2 * k + m % 3]

    def loading(m):
        k = m // 3
        return pltpu.make_async_copy(
            weights_in[m], straight.at[k] if m % 3 == 2 else raw.at[2 * k + m % 3], load.at[m]
        )

    load_tokens = pltpu.make_async_copy(tokens_h, tokens, load.at[6])
    load_merged = pltpu.make_async_copy(merged_h, merged, load.at[7])
    loading(0).start()
    loading(1).start()
    load_tokens.start()
    for m in (2, 3, 4, 5):
        loading(m).start()
    load_merged.start()

    barrier = pltpu.get_barrier_semaphore()
    targets = [inner, sibling] + to_peer[1:]
    for to in targets:
        pl.semaphore_signal(barrier, inc=1, device_id=to, device_id_type=pl.DeviceIdType.MESH)

    @on_mid
    def _():
        pl.semaphore_signal(barrier, inc=1, device_id=outer, device_id_type=pl.DeviceIdType.MESH)

    def turn(m):
        k = 2 * (m // 3) + m % 3
        loading(m).wait()
        for j in range(raw.shape[2] // 128):
            turned[k, j * 128:(j + 1) * 128, :] = raw[k, :, j * 128:(j + 1) * 128].T

    def lanes_of(zz, pp):
        return pl.ds(pl.multiple_of((zz * PLANE + pp) * ds, ds), ds)

    def p1(m, r):
        src = shard_of(m).at[pl.ds(pl.multiple_of(peers[r] * q, 16), q), :]
        return remote(src, w.at[m, :, lanes_of(z, p)], p1_s.at[m, r - 1], p1_r.at[m, r - 1], to_peer[r])

    def p1_in(m, r):
        src = w.at[m, :, lanes_of(z, peers[r])]
        return remote(src, src, p1_s.at[m, r - 1], p1_r.at[m, r - 1], to_peer[r])

    def start_p1(m):
        for r in (3, 1, 2):
            p1(m, r).start()
        w[m, :, lanes_of(z, p)] = shard_of(m)[pl.ds(pl.multiple_of(p * q, 16), q), :]

    def blk(m, zz):
        return w.at[m, :, pl.ds(pl.multiple_of(zz * pw, pw), pw)]

    first_slot = 3 * (1 - mid)

    def to_inner(m, r=None):
        at = blk(m, z) if r is None else w.at[m, :, lanes_of(z, peers[r])]
        return remote(at, at, z_s.at[m, 0], z_r.at[m, first_slot], inner)

    def to_outer(m, r=None):
        at = blk(m, z) if r is None else w.at[m, :, lanes_of(z, peers[r])]
        return remote(at, at, z_s.at[m, 1], z_r.at[m, 0], outer)

    def on_inner(m):
        return remote(blk(m, zo), blk(m, zo), z_s.at[m, 2], z_r.at[m, 1], inner)

    def on_outer(m, d):
        at = blk(m, z + d * toward)
        return remote(at, at, z_s.at[m, 2 + d], z_r.at[m, d], outer)

    def came(m, slot):
        zz = zo if slot == 3 else z + (slot + 1) * toward
        return remote(blk(m, zz), blk(m, zz), z_s.at[m, 0], z_r.at[m, slot], inner)

    def piece_out(m, r):
        to_inner(m, r).start()

        @on_mid
        def _():
            to_outer(m, r).start()

    def own_now(m):
        for r in (1, 2, 3):
            p1_in(m, r).wait_recv()
            piece_out(m, r)

    def own_inner(m):
        for r in (1, 2, 3):
            p1_in(m, r).wait_recv()
        to_inner(m).start()

    def own_outer(m):
        @on_mid
        def _():
            to_outer(m).start()

    def pass_in(m):
        @on_mid
        def _():
            came(m, 3).wait_recv()
            on_inner(m).start()

    def pass_out(m, d):
        @on_mid
        def _():
            came(m, d - 1).wait_recv()
            on_outer(m, d).start()

    def need(m, slot):
        @on_end
        def _():
            came(m, slot).wait_recv()

    bufs = (normed1, normed2)

    def piece(tt, h):
        return pl.ds(pl.multiple_of(tt * half + h * quarter, 16), quarter)

    def ag(f, r, h):
        at = piece(t, h)
        return remote(bufs[f].at[0, at, :], bufs[f].at[r, at, :], ag_s.at[f, r - 1, h], ag_r.at[f, r - 1, h], to_peer[r])

    def ag_on(f, h):
        at = piece(t, h)
        return remote(bufs[f].at[2 - h, at, :], bufs[f].at[3, at, :], ag_s.at[f, 2, h], ag_r.at[f, 2, h], to_peer[1 + h])

    def relay(f, r, h, tt):
        at = bufs[f].at[r, piece(tt, h), :]
        return remote(at, at, rel_s.at[f, r, h], rel_r.at[f, r, h], sibling)

    def ag_first(f):
        for r, h in ((2, 0), (1, 1)):
            ag(f, r, h).wait_recv()
            ag_on(f, h).start()
            relay(f, r, h, t).start()

    def ag_second(f):
        for r, h in ((2, 1), (1, 0)):
            ag(f, r, h).wait_recv()
            relay(f, r, h, t).start()

    def ag_far(f):
        for h in range(2):
            ag_on(f, h).wait_recv()
            relay(f, 3, h, t).start()

    zs = (z, zi, jnp.where(mid == 1, zo, z + 2 * toward), jnp.where(mid == 1, z + 2 * toward, z + 3 * toward))
    lanes = [pl.ds(pl.multiple_of(zz * pw, pw), pw) for zz in zs]
    lanes_a = pl.ds(pl.multiple_of((1 - low) * pw, pw), 3 * pw)
    lanes_b = pl.ds(pl.multiple_of(low * 3 * pw, pw), pw)
    first, second = pl.ds(0, quarter), pl.ds(quarter, quarter)

    def to_sibling(f, c, r):
        return remote(part.at[r, :, lanes[c]], sib.at[r, :, lanes[c]], sib_s.at[f, c, r], sib_r.at[f, c, r], sibling)

    def rs(f, c, kind):
        at = lanes[c]
        src, dst, r = (
            (comb.at[2, first, at], diag.at[0, :, at], 1),
            (comb.at[2, second, at], diag.at[1, :, at], 2),
            (comb.at[0, first, at], rsr.at[0, first, at], 1),
            (comb.at[0, second, at], rsr.at[0, second, at], 1),
            (comb.at[1, second, at], rsr.at[1, second, at], 2),
            (comb.at[1, first, at], rsr.at[1, first, at], 2),
        )[kind]
        return remote(src, dst, rs_s.at[f, c, kind], rs_r.at[f, c, kind], to_peer[r])

    def product(f, k, r, at):
        dims = (((1,), (1,)), ((), ()))
        return lax.dot_general(bufs[f][r, :, at], w[3 * f + k, :, at], dims, preferred_element_type=F32)

    def gate_start(f):
        @pl.loop(0, PLANE)
        def _(r):
            @pl.when(r > (0 if f == 0 else -1))
            def _():
                for h in range(2):
                    relay(f, r, h, 1 - t).wait_recv()

            acc_g[r] = product(f, 0, r, lanes_a)

    def up_start(f):
        @pl.loop(0, PLANE)
        def _(r):
            acc_u[r] = product(f, 1, r, lanes_a)

    def gate_end(f):
        @pl.loop(0, PLANE)
        def _(r):
            g = acc_g[r] + product(f, 0, r, lanes_b)
            acc_g[r] = g / (1.0 + jnp.exp(-g))

    def up_end(f):
        @pl.loop(0, PLANE)
        def _(r):
            u = acc_u[r] + product(f, 1, r, lanes_b)
            hidden[r] = (acc_g[r] * u).astype(BF16)

    def down(f, c):
        at = lanes[c]

        @pl.loop(0, PLANE)
        def _(k):
            r = PLANE - 1 - k
            part[r, :, at] = jnp.dot(hidden[r, other, :], w[3 * f + 2, :, at], preferred_element_type=F32).astype(BF16)
            to_sibling(f, c, r).start()
            own[r, :, at] = jnp.dot(hidden[r, mine, :], w[3 * f + 2, :, at], preferred_element_type=F32).astype(BF16)

        for r, kinds in ((3, (0, 1)), (1, (2,)), (2, (4,))):
            to_sibling(f, c, r).wait_recv()

            @pl.loop(0, half // (2 * step))
            def _(i):
                some = pl.ds(pl.multiple_of(i * 2 * step, step), 2 * step)
                comb[r - 1, some, at] = (own[r, some, at].astype(F32) + sib[r, some, at].astype(F32)).astype(BF16)

            for kind in kinds:
                rs(f, c, kind).start()
        to_sibling(f, c, 0).wait_recv()

    def finish(f, c):
        at = lanes[c]
        rs(f, c, 0).wait_recv()
        comb[1, first, at] = (comb[1, first, at].astype(F32) + diag[0, :, at].astype(F32)).astype(BF16)
        rs(f, c, 5).start()
        rs(f, c, 1).wait_recv()
        comb[0, second, at] = (comb[0, second, at].astype(F32) + diag[1, :, at].astype(F32)).astype(BF16)
        rs(f, c, 3).start()

    def reduced(rows_at, at):
        total = own[0, rows_at, at].astype(F32) + sib[0, rows_at, at].astype(F32)
        return total + rsr[0, rows_at, at].astype(F32) + rsr[1, rows_at, at].astype(F32)

    def out_across(c):
        return remote(out.at[mine, lanes[c]], out.at[mine, lanes[c]], fin_s.at[c], fin_r.at[c], sibling)

    def out_here(c, at):
        k = 0 if at is mine else 1
        return pltpu.make_async_copy(out.at[at, lanes[c]], out_h.at[at, lanes[c]], store.at[k, c])

    def land(f, c):
        for kind in (2, 4, 3, 5):
            rs(f, c, kind).wait_recv()
        at = lanes[c]

        @pl.loop(0, half // (2 * step))
        def _(i):
            some = pl.ds(pl.multiple_of(i * 2 * step, step), 2 * step)
            full = pl.ds(pl.multiple_of(t * half + i * 2 * step, step), 2 * step)
            if f == 0:
                value = tokens[full, at].astype(F32) + merged[full, at].astype(F32) + 0.5 * reduced(some, at)
                middle[some, at] = value
                squares = value * value
                sums = sum(squares[:, k * 128:(k + 1) * 128] for k in range(pw // 128))
                ssq[some, :] = sums if c == 0 else ssq[some, :] + sums
            else:
                out[full, at] = (middle[some, at] + 0.5 * reduced(some, at)).astype(BF16)

        if f == 1:
            out_across(c).start()
            out_here(c, mine).start()

    def norm_first(start, count):
        @pl.loop(0, count // step)
        def _(i):
            at = pl.ds(pl.multiple_of(start + i * step, step), step)
            normed1[0, at, :] = norm_rows(tokens[at, :].astype(F32), gain1[...]).astype(BF16)

    turn(0)
    pl.semaphore_wait(barrier, len(targets) + mid)
    start_p1(0)
    piece_out(0, 0)
    turn(1)
    start_p1(1)
    piece_out(1, 0)

    load_tokens.wait()
    for h in range(2):
        norm_first(t * half + h * quarter, quarter)
        ag(0, 2 - h, h).start()
        ag(0, 1 + h, h).start()
    loading(2).wait()
    start_p1(2)
    own_now(0)
    norm_first((1 - t) * half, half)
    own_now(1)
    turn(3)
    turn(4)
    pass_in(0)
    pass_out(0, 1)
    ag_first(0)
    loading(5).wait()
    for m in (3, 4, 5):
        start_p1(m)
    pass_in(1)
    pass_out(1, 1)
    ag_second(0)
    pass_out(0, 2)
    own_inner(2)
    pass_out(1, 2)
    own_outer(2)
    ag_far(0)

    for slot in (0, 1):
        need(0, slot)
    gate_start(0)
    for slot in (0, 1):
        need(1, slot)
    up_start(0)
    pass_in(2)
    pass_out(2, 1)
    need(0, 2)
    gate_end(0)
    need(1, 2)
    up_end(0)
    down(0, 0)
    own_inner(3)
    need(2, 0)
    down(0, 1)
    finish(0, 0)
    need(2, 1)
    down(0, 2)
    finish(0, 1)
    pass_out(2, 2)
    own_outer(3)
    own_inner(4)
    own_inner(5)
    load_merged.wait()
    land(0, 0)
    need(2, 2)
    down(0, 3)
    finish(0, 2)
    land(0, 1)
    pass_in(3)
    pass_out(3, 1)
    finish(0, 3)
    land(0, 2)
    land(0, 3)

    for h in range(2):
        @pl.loop(0, quarter // step)
        def _(i):
            at = pl.ds(pl.multiple_of(h * quarter + i * step, step), step)
            full = pl.ds(pl.multiple_of(t * half + h * quarter + i * step, step), step)
            scale = lax.rsqrt(jnp.sum(ssq[at, :], axis=-1, keepdims=True) / width + EPS)
            normed2[0, full, :] = (middle[at, :] * scale * gain2[...]).astype(BF16)

        ag(1, 2 - h, h).start()
        ag(1, 1 + h, h).start()
        relay(1, 0, h, t).start()

    pass_out(3, 2)
    own_outer(4)
    pass_in(4)
    pass_out(4, 1)
    ag_first(1)
    pass_out(4, 2)
    own_outer(5)
    pass_in(5)
    pass_out(5, 1)
    ag_second(1)
    pass_out(5, 2)
    ag_far(1)

    for slot in (0, 1):
        need(3, slot)
    gate_start(1)
    for slot in (0, 1):
        need(4, slot)
    up_start(1)
    need(3, 2)
    gate_end(1)
    need(4, 2)
    up_end(1)
    for c in range(LINE):
        for r in range(PLANE):
            to_sibling(0, c, r).wait_send()
        for kind in range(6):
            rs(0, c, kind).wait_send()
    down(1, 0)
    need(5, 0)
    down(1, 1)
    finish(1, 0)
    need(5, 1)
    down(1, 2)
    finish(1, 1)
    land(1, 0)
    need(5, 2)
    down(1, 3)
    finish(1, 2)
    land(1, 1)
    finish(1, 3)
    land(1, 2)
    land(1, 3)

    for m in range(6):
        for r in (1, 2, 3):
            p1(m, r).wait_send()
        to_inner(m).wait_send()

        @on_mid
        def _():
            to_outer(m).wait_send()
            on_inner(m).wait_send()
            on_outer(m, 1).wait_send()
            on_outer(m, 2).wait_send()

    for f in range(2):
        for h in range(2):
            for r in (1, 2):
                ag(f, r, h).wait_send()
            ag_on(f, h).wait_send()
            for r in range(1 - f, PLANE):
                relay(f, r, h, t).wait_send()
    for c in range(LINE):
        for r in range(PLANE):
            to_sibling(1, c, r).wait_send()
        for kind in range(6):
            rs(1, c, kind).wait_send()
    theirs = [remote(out.at[other, lanes[c]], out.at[other, lanes[c]], fin_s.at[c], fin_r.at[c], sibling) for c in range(LINE)]
    for c in range(LINE):
        theirs[c].wait_recv()
        out_here(c, other).start()
    for c in range(LINE):
        out_across(c).wait_send()
        out_here(c, mine).wait()
        out_here(c, other).wait()


def plane_shards(tokens, merged, gain1, g1, u1, d1, gain2, g2, u2, d2):
    rows, width = tokens.shape
    half = rows // 2
    hid, ds = d1.shape
    q = hid // PLANE
    vmem = pl.BlockSpec(memory_space=pltpu.VMEM)
    far = pl.BlockSpec(memory_space=pl.ANY)
    dma = lambda *s: pltpu.SemaphoreType.DMA(s)
    return pl.pallas_call(
        kernel,
        out_shape=jax.ShapeDtypeStruct((rows, width), BF16),
        in_specs=[far, far, vmem, vmem] + [far] * 6,
        out_specs=far,
        scratch_shapes=[
            pltpu.VMEM((4, ds, hid), BF16),
            pltpu.VMEM((4, hid, ds), BF16),
            pltpu.VMEM((2, hid, ds), BF16),
            pltpu.VMEM((rows, width), BF16),
            pltpu.VMEM((rows, width), BF16),
            pltpu.VMEM((rows, width), BF16),
            pltpu.VMEM((6, q, width), BF16),
            pltpu.VMEM((PLANE, rows, width), BF16),
            pltpu.VMEM((PLANE, rows, width), BF16),
            pltpu.VMEM((PLANE, rows, q), F32),
            pltpu.VMEM((PLANE, rows, q), F32),
            pltpu.VMEM((PLANE, rows, q), BF16),
            pltpu.VMEM((PLANE, half, width), BF16),
            pltpu.VMEM((PLANE, half, width), BF16),
            pltpu.VMEM((PLANE, half, width), BF16),
            pltpu.VMEM((PLANE - 1, half, width), BF16),
            pltpu.VMEM((2, half // 2, width), BF16),
            pltpu.VMEM((2, half, width), BF16),
            pltpu.VMEM((half, width), F32),
            pltpu.VMEM((half, 128), F32),
            dma(8), dma(6, 3), dma(6, 3), dma(6, 5), dma(6, 4),
            dma(2, 3, 2), dma(2, 3, 2), dma(2, 4, 2), dma(2, 4, 2),
            dma(2, LINE, 4), dma(2, LINE, 4), dma(2, LINE, 6), dma(2, LINE, 6),
            dma(LINE), dma(LINE), dma(2, LINE),
        ],
        compiler_params=pltpu.CompilerParams(
            collective_id=0, has_side_effects=True, vmem_limit_bytes=60 * 2**20
        ),
    )(tokens, merged, gain1[None], gain2[None], g1, u1, d1, g2, u2, d2)


def shards(n_fs, n_tp, *args):
    rows, width = args[0].shape
    hid, cols = args[5].shape
    fits = n_fs == PLANE * LINE and n_tp == 2 and cols % 128 == 0
    fits = fits and hid % (32 * PLANE) == 0 and rows % 64 == 0
    return plane_shards(*args) if fits else gathered_shards(*args)


def solution(mesh):
    return jax.shard_map(
        functools.partial(shards, mesh.shape["fs"], mesh.shape["tp"]),
        mesh=mesh,
        in_specs=(
            P("fs", None),
            P("fs", None),
            P(),
            P("fs", "tp"),
            P("fs", "tp"),
            P("tp", "fs"),
            P(),
            P("fs", "tp"),
            P("fs", "tp"),
            P("tp", "fs"),
        ),
        out_specs=P("fs", None),
        check_vma=False,
    )
```

time: 202 us -> 168 us (0.83)
  Pallas kernels: 194 us -> 164 us
  local copies, waits for them, and re-layouts: 8.42 us -> 2.73 us
    pallas_call x1, Pallas kernels: 194 us -> 164 us  [plane_shards(): pl.pallas_call(kernel, out_shape=jax.ShapeDtypeStruct((rows, width), BF16...]
    unnamed x9 -> x1, local copies, waits for them, and re-layouts: 8.42 us -> 2.73 us
where the time goes in v1:
time: 168 us; the launch traced here: 167 us
  Pallas kernels  164 us (98%)
  local copies, waits for them, and re-layouts  2.73 us (2%)
    pallas_call x1, Pallas kernels, plane_shards(): pl.pallas_call(kernel, out_shape=jax.ShapeDtypeStruct((rows, width), BF16...  164 us

profile of v1, /device:TPU:0, one launch (start us, length us, event | category | flops | bytes accessed | tf_op | source)
XLA Modules:
  0.0 167.2 jit_solution(17679094108801862660)
XLA Ops:
  0.0 164.5 %shard_map.100 = bf16[384,2048]{1,0:T(8,128)(2,1)} custom-call(bf16[384,2048]{1,0:T(8,128)(2,1)} %tokens_h.1, bf16[384,2048]{1,0:T(8,128)(2,1)} %merged_h.1, f32[1,2048]{1,0:T(1,128)} %bitcast.2, f32[1,2048]{1,0:T(1,128)} %bitcast.3, bf16[128,1408]{1,0:T(8,128)(2,1)} %wa.1, bf16[128,1408]{1,0:T(8,128)(2,1)} %wb.1, bf16[1408,128]{1,0:T(8,128)(2,1)} %wc.1, ...), custom_call_target="tpu_custom_call" | custom-call | tf_op jit(solution)/shard_map/pallas_call | solution.py:526
  164.5 2.7 %copy.12 = bf16[384,2048]{1,0:T(8,128)(2,1)} copy(bf16[384,2048]{1,0:T(8,128)(2,1)} %shard_map.100) | data formatting | bytes 3145728

commit v2 on v1

--- a/solution.py
+++ b/solution.py
@@ -40,11 +40,11 @@
 
 
 def kernel(
-    tokens_h, merged_h, gain1, gain2, wa, wb, wc, wd, we, wf, out_h,
-    raw, turned, straight, tokens, merged, out, w, normed1, normed2, acc_g, acc_u, hidden,
+    tokens_h, merged_h, gain1_h, gain2_h, wa, wb, wc, wd, we, wf, out,
+    raw, turned, straight, tokens, merged, gain1, gain2, fin, w, normed1, normed2, acc_g, acc_u, hidden,
     part, own, sib, comb, diag, rsr, middle, ssq,
     load, p1_s, p1_r, z_s, z_r,
-    ag_s, ag_r, rel_s, rel_r, sib_s, sib_r, rs_s, rs_r, fin_s, fin_r, store,
+    ag_s, ag_r, rel_s, rel_r, sib_s, sib_r, rs_s, rs_r, fin_s, fin_r,
 ):
     weights_in = (wa, wb, wc, wd, we, wf)
     fs = lax.axis_index("fs")
@@ -98,12 +98,16 @@
 
     load_tokens = pltpu.make_async_copy(tokens_h, tokens, load.at[6])
     load_merged = pltpu.make_async_copy(merged_h, merged, load.at[7])
-    loading(0).start()
-    loading(1).start()
+    load_gain1 = pltpu.make_async_copy(gain1_h, gain1, load.at[8])
+    load_gain2 = pltpu.make_async_copy(gain2_h, gain2, load.at[9])
+    for m in (2, 0, 1):
+        loading(m).start()
     load_tokens.start()
-    for m in (2, 3, 4, 5):
+    load_gain1.start()
+    for m in (5, 3, 4):
         loading(m).start()
     load_merged.start()
+    load_gain2.start()
 
     barrier = pltpu.get_barrier_semaphore()
     targets = [inner, sibling] + to_peer[1:]
@@ -131,10 +135,12 @@
         src = w.at[m, :, lanes_of(z, peers[r])]
         return remote(src, src, p1_s.at[m, r - 1], p1_r.at[m, r - 1], to_peer[r])
 
+    def place(m):
+        w[m, :, lanes_of(z, p)] = shard_of(m)[pl.ds(pl.multiple_of(p * q, 16), q), :]
+
     def start_p1(m):
         for r in (3, 1, 2):
             p1(m, r).start()
-        w[m, :, lanes_of(z, p)] = shard_of(m)[pl.ds(pl.multiple_of(p * q, 16), q), :]
 
     def blk(m, zz):
         return w.at[m, :, pl.ds(pl.multiple_of(zz * pw, pw), pw)]
@@ -155,6 +161,10 @@
     def on_outer(m, d):
         at = blk(m, z + d * toward)
         return remote(at, at, z_s.at[m, 2 + d], z_r.at[m, d], outer)
+
+    def last_half(k):
+        at = w.at[5, :, pl.ds(pl.multiple_of((z + (3 - mid) * toward) * pw + k * pw // 2, pw // 2), pw // 2)]
+        return remote(at, at, z_s.at[5, 4 + k], z_r.at[5, (2, 4)[k]], outer)
 
     def came(m, slot):
         zz = zo if slot == 3 else z + (slot + 1) * toward
@@ -172,15 +182,22 @@
             p1_in(m, r).wait_recv()
             piece_out(m, r)
 
-    def own_inner(m):
+    def own_inner(m, begun=False):
         for r in (1, 2, 3):
             p1_in(m, r).wait_recv()
-        to_inner(m).start()
-
-    def own_outer(m):
+            if begun:
+                to_inner(m, r).start()
+        if not begun:
+            to_inner(m).start()
+
+    def own_outer(m, begun=False):
         @on_mid
         def _():
-            to_outer(m).start()
+            if begun:
+                for r in (1, 2, 3):
+                    to_outer(m, r).start()
+            else:
+                to_outer(m).start()
 
     def pass_in(m):
         @on_mid
@@ -232,17 +249,25 @@
             ag_on(f, h).wait_recv()
             relay(f, 3, h, t).start()
 
+    def need_half(k):
+        @on_end
+        def _():
+            last_half(k).wait_recv()
+
     zs = (z, zi, jnp.where(mid == 1, zo, z + 2 * toward), jnp.where(mid == 1, z + 2 * toward, z + 3 * toward))
-    lanes = [pl.ds(pl.multiple_of(zz * pw, pw), pw) for zz in zs]
+    hw = pw // 2
+    widths = ((pw,) * LINE, (pw,) * (LINE - 1) + (hw, hw))
+    lanes = [[pl.ds(pl.multiple_of(zz * pw, pw), pw) for zz in zs]]
+    lanes.append(lanes[0][:-1] + [pl.ds(pl.multiple_of(zs[-1] * pw + k * hw, hw), hw) for k in range(2)])
     lanes_a = pl.ds(pl.multiple_of((1 - low) * pw, pw), 3 * pw)
     lanes_b = pl.ds(pl.multiple_of(low * 3 * pw, pw), pw)
     first, second = pl.ds(0, quarter), pl.ds(quarter, quarter)
 
     def to_sibling(f, c, r):
-        return remote(part.at[r, :, lanes[c]], sib.at[r, :, lanes[c]], sib_s.at[f, c, r], sib_r.at[f, c, r], sibling)
+        return remote(part.at[r, :, lanes[f][c]], sib.at[r, :, lanes[f][c]], sib_s.at[f, c, r], sib_r.at[f, c, r], sibling)
 
     def rs(f, c, kind):
-        at = lanes[c]
+        at = lanes[f][c]
         src, dst, r = (
             (comb.at[2, first, at], diag.at[0, :, at], 1),
             (comb.at[2, second, at], diag.at[1, :, at], 2),
@@ -257,44 +282,58 @@
         dims = (((1,), (1,)), ((), ()))
         return lax.dot_general(bufs[f][r, :, at], w[3 * f + k, :, at], dims, preferred_element_type=F32)
 
-    def gate_start(f):
-        @pl.loop(0, PLANE)
-        def _(r):
-            @pl.when(r > (0 if f == 0 else -1))
-            def _():
-                for h in range(2):
-                    relay(f, r, h, 1 - t).wait_recv()
-
-            acc_g[r] = product(f, 0, r, lanes_a)
-
-    def up_start(f):
-        @pl.loop(0, PLANE)
-        def _(r):
-            acc_u[r] = product(f, 1, r, lanes_a)
-
-    def gate_end(f):
-        @pl.loop(0, PLANE)
-        def _(r):
-            g = acc_g[r] + product(f, 0, r, lanes_b)
-            acc_g[r] = g / (1.0 + jnp.exp(-g))
-
-    def up_end(f):
-        @pl.loop(0, PLANE)
-        def _(r):
-            u = acc_u[r] + product(f, 1, r, lanes_b)
-            hidden[r] = (acc_g[r] * u).astype(BF16)
+    def slot_in(f, r):
+        @pl.when(r > (0 if f == 0 else -1))
+        def _():
+            for h in range(2):
+                relay(f, r, h, 1 - t).wait_recv()
+
+    def silu(g):
+        return g / (1.0 + jnp.exp(-g))
+
+    def make_hidden(f):
+        every = slice(None)
+
+        @on_mid
+        def _():
+            @pl.loop(0, PLANE)
+            def _(r):
+                slot_in(f, r)
+                g = silu(product(f, 0, r, every))
+                hidden[r] = (g * product(f, 1, r, every)).astype(BF16)
+
+        @on_end
+        def _():
+            for m, slot in ((0, 0), (0, 1), (0, 2), (1, 0), (1, 1)):
+                came(3 * f + m, slot).wait_recv()
+
+            @pl.loop(0, PLANE)
+            def _(r):
+                slot_in(f, r)
+                acc_g[r] = silu(product(f, 0, r, every))
+                acc_u[r] = product(f, 1, r, lanes_a)
+
+            came(3 * f + 1, 2).wait_recv()
+
+            @pl.loop(0, PLANE)
+            def _(r):
+                u = acc_u[r] + product(f, 1, r, lanes_b)
+                hidden[r] = (acc_g[r] * u).astype(BF16)
 
     def down(f, c):
-        at = lanes[c]
+        at = lanes[f][c]
+
+        def part_of(r, rows_at):
+            return jnp.dot(hidden[r, rows_at, :], w[3 * f + 2, :, at], preferred_element_type=F32).astype(BF16)
 
         @pl.loop(0, PLANE)
         def _(k):
             r = PLANE - 1 - k
-            part[r, :, at] = jnp.dot(hidden[r, other, :], w[3 * f + 2, :, at], preferred_element_type=F32).astype(BF16)
+            part[r, :, at] = part_of(r, other)
             to_sibling(f, c, r).start()
-            own[r, :, at] = jnp.dot(hidden[r, mine, :], w[3 * f + 2, :, at], preferred_element_type=F32).astype(BF16)
-
-        for r, kinds in ((3, (0, 1)), (1, (2,)), (2, (4,))):
+
+        for r, kinds in ((3, (0, 1)), (2, (4,)), (1, (2,))):
+            own[r, :, at] = part_of(r, mine)
             to_sibling(f, c, r).wait_recv()
 
             @pl.loop(0, half // (2 * step))
@@ -304,10 +343,11 @@
 
             for kind in kinds:
                 rs(f, c, kind).start()
+        own[0, :, at] = part_of(0, mine)
         to_sibling(f, c, 0).wait_recv()
 
     def finish(f, c):
-        at = lanes[c]
+        at = lanes[f][c]
         rs(f, c, 0).wait_recv()
         comb[1, first, at] = (comb[1, first, at].astype(F32) + diag[0, :, at].astype(F32)).astype(BF16)
         rs(f, c, 5).start()
@@ -320,16 +360,13 @@
         return total + rsr[0, rows_at, at].astype(F32) + rsr[1, rows_at, at].astype(F32)
 
     def out_across(c):
-        return remote(out.at[mine, lanes[c]], out.at[mine, lanes[c]], fin_s.at[c], fin_r.at[c], sibling)
-
-    def out_here(c, at):
-        k = 0 if at is mine else 1
-        return pltpu.make_async_copy(out.at[at, lanes[c]], out_h.at[at, lanes[c]], store.at[k, c])
+        at = lanes[1][c]
+        return remote(out.at[mine, at], fin.at[:, at], fin_s.at[c], fin_r.at[c], sibling)
 
     def land(f, c):
         for kind in (2, 4, 3, 5):
             rs(f, c, kind).wait_recv()
-        at = lanes[c]
+        at = lanes[f][c]
 
         @pl.loop(0, half // (2 * step))
         def _(i):
@@ -339,14 +376,13 @@
                 value = tokens[full, at].astype(F32) + merged[full, at].astype(F32) + 0.5 * reduced(some, at)
                 middle[some, at] = value
                 squares = value * value
-                sums = sum(squares[:, k * 128:(k + 1) * 128] for k in range(pw // 128))
+                sums = sum(squares[:, k * 128:(k + 1) * 128] for k in range(widths[f][c] // 128))
                 ssq[some, :] = sums if c == 0 else ssq[some, :] + sums
             else:
                 out[full, at] = (middle[some, at] + 0.5 * reduced(some, at)).astype(BF16)
 
         if f == 1:
             out_across(c).start()
-            out_here(c, mine).start()
 
     def norm_first(start, count):
         @pl.loop(0, count // step)
@@ -354,20 +390,28 @@
             at = pl.ds(pl.multiple_of(start + i * step, step), step)
             normed1[0, at, :] = norm_rows(tokens[at, :].astype(F32), gain1[...]).astype(BF16)
 
+    loading(2).wait()
+    place(2)
+    pl.semaphore_wait(barrier, len(targets) + mid)
+    piece_out(2, 0)
     turn(0)
-    pl.semaphore_wait(barrier, len(targets) + mid)
     start_p1(0)
+    place(0)
     piece_out(0, 0)
     turn(1)
     start_p1(1)
+    place(1)
     piece_out(1, 0)
+    loading(5).wait()
+    place(5)
+    piece_out(5, 0)
 
     load_tokens.wait()
+    load_gain1.wait()
     for h in range(2):
         norm_first(t * half + h * quarter, quarter)
         ag(0, 2 - h, h).start()
         ag(0, 1 + h, h).start()
-    loading(2).wait()
     start_p1(2)
     own_now(0)
     norm_first((1 - t) * half, half)
@@ -377,30 +421,22 @@
     pass_in(0)
     pass_out(0, 1)
     ag_first(0)
-    loading(5).wait()
     for m in (3, 4, 5):
         start_p1(m)
+    place(3)
+    place(4)
     pass_in(1)
     pass_out(1, 1)
     ag_second(0)
     pass_out(0, 2)
-    own_inner(2)
+    own_inner(2, True)
     pass_out(1, 2)
-    own_outer(2)
+    own_outer(2, True)
     ag_far(0)
 
-    for slot in (0, 1):
-        need(0, slot)
-    gate_start(0)
-    for slot in (0, 1):
-        need(1, slot)
-    up_start(0)
+    make_hidden(0)
     pass_in(2)
     pass_out(2, 1)
-    need(0, 2)
-    gate_end(0)
-    need(1, 2)
-    up_end(0)
     down(0, 0)
     own_inner(3)
     need(2, 0)
@@ -412,8 +448,9 @@
     pass_out(2, 2)
     own_outer(3)
     own_inner(4)
-    own_inner(5)
+    own_inner(5, True)
     load_merged.wait()
+    load_gain2.wait()
     land(0, 0)
     need(2, 2)
     down(0, 3)
@@ -443,23 +480,20 @@
     pass_out(4, 1)
     ag_first(1)
     pass_out(4, 2)
-    own_outer(5)
+    own_outer(5, True)
     pass_in(5)
     pass_out(5, 1)
     ag_second(1)
-    pass_out(5, 2)
+
+    @on_mid
+    def _():
+        came(5, 1).wait_recv()
+        for k in range(2):
+            last_half(k).start()
+
     ag_far(1)
 
-    for slot in (0, 1):
-        need(3, slot)
-    gate_start(1)
-    for slot in (0, 1):
-        need(4, slot)
-    up_start(1)
-    need(3, 2)
-    gate_end(1)
-    need(4, 2)
-    up_end(1)
+    make_hidden(1)
     for c in range(LINE):
         for r in range(PLANE):
             to_sibling(0, c, r).wait_send()
@@ -473,13 +507,17 @@
     down(1, 2)
     finish(1, 1)
     land(1, 0)
-    need(5, 2)
+    need_half(0)
     down(1, 3)
     finish(1, 2)
     land(1, 1)
+    need_half(1)
+    down(1, 4)
     finish(1, 3)
     land(1, 2)
+    finish(1, 4)
     land(1, 3)
+    land(1, 4)
 
     for m in range(6):
         for r in (1, 2, 3):
@@ -491,7 +529,11 @@
             to_outer(m).wait_send()
             on_inner(m).wait_send()
             on_outer(m, 1).wait_send()
-            on_outer(m, 2).wait_send()
+            if m < 5:
+                on_outer(m, 2).wait_send()
+            else:
+                last_half(0).wait_send()
+                last_half(1).wait_send()
 
     for f in range(2):
         for h in range(2):
@@ -500,19 +542,17 @@
             ag_on(f, h).wait_send()
             for r in range(1 - f, PLANE):
                 relay(f, r, h, t).wait_send()
-    for c in range(LINE):
+    for c in range(LINE + 1):
         for r in range(PLANE):
             to_sibling(1, c, r).wait_send()
         for kind in range(6):
             rs(1, c, kind).wait_send()
-    theirs = [remote(out.at[other, lanes[c]], out.at[other, lanes[c]], fin_s.at[c], fin_r.at[c], sibling) for c in range(LINE)]
-    for c in range(LINE):
-        theirs[c].wait_recv()
-        out_here(c, other).start()
-    for c in range(LINE):
+    for c in range(LINE + 1):
+        out_across(c).wait_recv()
+        at = lanes[1][c]
+        out[other, at] = fin[:, at]
+    for c in range(LINE + 1):
         out_across(c).wait_send()
-        out_here(c, mine).wait()
-        out_here(c, other).wait()
 
 
 def plane_shards(tokens, merged, gain1, g1, u1, d1, gain2, g2, u2, d2):
@@ -520,21 +560,22 @@
     half = rows // 2
     hid, ds = d1.shape
     q = hid // PLANE
-    vmem = pl.BlockSpec(memory_space=pltpu.VMEM)
     far = pl.BlockSpec(memory_space=pl.ANY)
     dma = lambda *s: pltpu.SemaphoreType.DMA(s)
     return pl.pallas_call(
         kernel,
-        out_shape=jax.ShapeDtypeStruct((rows, width), BF16),
-        in_specs=[far, far, vmem, vmem] + [far] * 6,
-        out_specs=far,
+        out_shape=pltpu.VMEM((rows, width), BF16),
+        in_specs=[far] * 10,
+        out_specs=pl.BlockSpec(memory_space=pltpu.VMEM),
         scratch_shapes=[
             pltpu.VMEM((4, ds, hid), BF16),
             pltpu.VMEM((4, hid, ds), BF16),
             pltpu.VMEM((2, hid, ds), BF16),
             pltpu.VMEM((rows, width), BF16),
             pltpu.VMEM((rows, width), BF16),
-            pltpu.VMEM((rows, width), BF16),
+            pltpu.VMEM((1, width), F32),
+            pltpu.VMEM((1, width), F32),
+            pltpu.VMEM((half, width), BF16),
             pltpu.VMEM((6, q, width), BF16),
             pltpu.VMEM((PLANE, rows, width), BF16),
             pltpu.VMEM((PLANE, rows, width), BF16),
@@ -549,10 +590,10 @@
             pltpu.VMEM((2, half, width), BF16),
             pltpu.VMEM((half, width), F32),
             pltpu.VMEM((half, 128), F32),
-            dma(8), dma(6, 3), dma(6, 3), dma(6, 5), dma(6, 4),
+            dma(10), dma(6, 3), dma(6, 3), dma(6, 6), dma(6, 5),
             dma(2, 3, 2), dma(2, 3, 2), dma(2, 4, 2), dma(2, 4, 2),
-            dma(2, LINE, 4), dma(2, LINE, 4), dma(2, LINE, 6), dma(2, LINE, 6),
-            dma(LINE), dma(LINE), dma(2, LINE),
+            dma(2, LINE + 1, 4), dma(2, LINE + 1, 4), dma(2, LINE + 1, 6), dma(2, LINE + 1, 6),
+            dma(LINE + 1), dma(LINE + 1),
         ],
         compiler_params=pltpu.CompilerParams(
             collective_id=0, has_side_effects=True, vmem_limit_bytes=60 * 2**20

time: 168 us -> 163 us (0.970)
  Pallas kernels: 164 us -> 162 us
    pallas_call x1, Pallas kernels: 164 us -> 162 us  [plane_shards(): pl.pallas_call(kernel, out_shape=pltpu.VMEM((rows, width), BF16), in_spec...]
where the time goes in v2:
time: 163 us
  Pallas kernels  162 us (99%)
    pallas_call x1, Pallas kernels, plane_shards(): pl.pallas_call(kernel, out_shape=pltpu.VMEM((rows, width), BF16), in_spec...  162 us

profile of v2, /device:TPU:0, one launch (start us, length us, event | category | flops | bytes accessed | tf_op | source)
XLA Modules:
  0.0 162.7 jit_solution(4254301329363024107)
XLA Ops:
  0.0 161.6 %shard_map.100 = bf16[384,2048]{1,0:T(8,128)(2,1)S(1)} custom-call(bf16[384,2048]{1,0:T(8,128)(2,1)} %tokens_h.1, bf16[384,2048]{1,0:T(8,128)(2,1)} %merged_h.1, f32[1,2048]{1,0:T(1,128)} %bitcast.2, f32[1,2048]{1,0:T(1,128)} %bitcast.3, bf16[128,1408]{1,0:T(8,128)(2,1)} %wa.1, bf16[128,1408]{1,0:T(8,128)(2,1)} %wb.1, bf16[1408,128]{1,0:T(8,128)(2,1)} %wc.1, ...), custom_call_target="tpu_custom_call" | custom-call | tf_op jit(solution)/shard_map/pallas_call | solution.py:565
  161.6 1.1 copy.12

commit v3 on v1

v3 whole, which is shorter than its diff:
```python
import functools

import jax
import jax.numpy as jnp
from jax import lax
from jax.experimental import pallas as pl
from jax.experimental.pallas import tpu as pltpu
from jax.sharding import PartitionSpec as P

EPS = 1e-06
BF16 = jnp.bfloat16
F32 = jnp.float32
PLANE = 4
LINE = 4
PARTS = 2


def norm_rows(values, gain):
    scale = lax.rsqrt(jnp.mean(values * values, axis=-1, keepdims=True) + EPS)
    return values * scale * gain


def gathered_block(normed, gate, up, down):
    gate_whole = lax.all_gather(gate, "fs", axis=0, tiled=True)
    up_whole = lax.all_gather(up, "fs", axis=0, tiled=True)
    g = jnp.dot(normed, gate_whole, preferred_element_type=F32)
    u = jnp.dot(normed, up_whole, preferred_element_type=F32)
    hidden = (jax.nn.silu(g) * u).astype(BF16)
    down_whole = lax.all_gather(down, "fs", axis=1, tiled=True)
    part = jnp.dot(hidden, down_whole, preferred_element_type=F32)
    return lax.psum(part.astype(BF16), "tp").astype(F32)


def gathered_shards(tokens, merged, gain1, g1, u1, d1, gain2, g2, u2, d2):
    source = tokens.astype(F32)
    middle = source + merged.astype(F32)
    normed = norm_rows(source, gain1).astype(BF16)
    middle = middle + 0.5 * gathered_block(normed, g1, u1, d1)
    normed = norm_rows(middle, gain2).astype(BF16)
    return (middle + 0.5 * gathered_block(normed, g2, u2, d2)).astype(BF16)


def kernel(
    tokens_h, merged_h, gain1_h, gain2_h, wa, wb, wc, wd, we, wf, out_h,
    raw, turned, straight, tokens, merged, gain1, gain2, here, fin, w, normed1, normed2, acc_g, acc_u, hidden,
    prod, sib, comb, diag, rsr, middle, ssq,
    load, p1_s, p1_r, z_s, z_r,
    ag_s, ag_r, rel_s, rel_r, sib_s, sib_r, rs_s, rs_r, fin_s, fin_r, store,
):
    weights_in = (wa, wb, wc, wd, we, wf)
    fs = lax.axis_index("fs")
    t = lax.axis_index("tp")
    z = fs // PLANE
    p = fs % PLANE
    rows, width = tokens.shape
    half = rows // 2
    quarter = half // 2
    q, pw = w.shape[1], width // LINE
    ds = wc.shape[1]
    step = 16

    def dev(zz, pp, tt):
        return {"fs": zz * PLANE + pp, "tp": tt}

    peers = (p, p + 1 - 2 * (p % 2), (p + 2) % PLANE, PLANE - 1 - p)
    to_peer = [dev(z, pp, t) for pp in peers]
    sibling = dev(z, p, 1 - t)

    low = (z < 2).astype(jnp.int32)
    toward = 2 * low - 1
    mid = (z % 3 != 0).astype(jnp.int32)
    zi, zo = z + toward, z - toward * mid
    inner, outer = dev(zi, p, t), dev(zo, p, t)

    def on_mid(f):
        pl.when(mid == 1)(f)

    def on_end(f):
        pl.when(mid == 0)(f)

    def remote(src, dst, s, r, to):
        return pltpu.make_async_remote_copy(
            src_ref=src, dst_ref=dst, send_sem=s, recv_sem=r,
            device_id=to, device_id_type=pl.DeviceIdType.MESH,
        )

    mine = pl.ds(pl.multiple_of(t * half, 16), half)
    other = pl.ds(pl.multiple_of((1 - t) * half, 16), half)

    def shard_of(m):
        k = m // 3
        return straight.at[k] if m % 3 == 2 else turned.at[2 * k + m % 3]

    def loading(m):
        k = m // 3
        return pltpu.make_async_copy(
            weights_in[m], straight.at[k] if m % 3 == 2 else raw.at[2 * k + m % 3], load.at[m]
        )

    load_tokens = pltpu.make_async_copy(tokens_h, tokens, load.at[6])
    load_merged = pltpu.make_async_copy(merged_h, merged, load.at[7])
    load_gain1 = pltpu.make_async_copy(gain1_h, gain1, load.at[8])
    load_gain2 = pltpu.make_async_copy(gain2_h, gain2, load.at[9])
    for m in (0, 1):
        loading(m).start()
    load_tokens.start()
    load_gain1.start()
    for m in (2, 3, 4, 5):
        loading(m).start()
    load_merged.start()
    load_gain2.start()

    barrier = pltpu.get_barrier_semaphore()
    targets = [inner, sibling] + to_peer[1:]
    for to in targets:
        pl.semaphore_signal(barrier, inc=1, device_id=to, device_id_type=pl.DeviceIdType.MESH)

    @on_mid
    def _():
        pl.semaphore_signal(barrier, inc=1, device_id=outer, device_id_type=pl.DeviceIdType.MESH)

    def turn(m):
        k = 2 * (m // 3) + m % 3
        loading(m).wait()
        for j in range(raw.shape[2] // 128):
            turned[k, j * 128:(j + 1) * 128, :] = raw[k, :, j * 128:(j + 1) * 128].T

    def lanes_of(zz, pp):
        return pl.ds(pl.multiple_of((zz * PLANE + pp) * ds, ds), ds)

    def p1_sem(m, r):
        return p1_r.at[3 * m + r - 1 if m < 2 else 4 + m]

    def p1(m, r):
        src = shard_of(m).at[pl.ds(pl.multiple_of(peers[r] * q, 16), q), :]
        return remote(src, w.at[m, :, lanes_of(z, p)], p1_s.at[0], p1_sem(m, r), to_peer[r])

    def p1_in(m, r):
        src = w.at[m, :, lanes_of(z, peers[r])]
        return remote(src, src, p1_s.at[0], p1_sem(m, r), to_peer[r])

    def p1_whole(m):
        src = w.at[m, :, pl.ds(0, (PLANE - 1) * ds)]
        return remote(src, src, p1_s.at[0], p1_sem(m, 1), to_peer[1])

    def place(m):
        w[m, :, lanes_of(z, p)] = shard_of(m)[pl.ds(pl.multiple_of(p * q, 16), q), :]

    def start_p1(m):
        for r in (3, 1, 2):
            p1(m, r).start()

    def blk(m, zz):
        return w.at[m, :, pl.ds(pl.multiple_of(zz * pw, pw), pw)]

    first_slot = 3 * (1 - mid)
    wide = 1 + 3 * PARTS

    def z_sem(m, slot):
        return z_r.at[4 * m + (m // 3) * (wide - 4) + slot]

    def to_inner(m, r=None):
        at = blk(m, z) if r is None else w.at[m, :, lanes_of(z, peers[r])]
        return remote(at, at, z_s.at[0], z_sem(m, first_slot), inner)

    def to_outer(m, r):
        at = w.at[m, :, lanes_of(z, peers[r])]
        return remote(at, at, z_s.at[1], z_sem(m, 0), outer)

    def on_inner(m):
        return remote(blk(m, zo), blk(m, zo), z_s.at[0], z_sem(m, 1), inner)

    def cuts(m):
        return PARTS if m % 3 == 2 else 1

    def part_blk(m, zz, k):
        n = pw // cuts(m)
        return w.at[m, :, pl.ds(pl.multiple_of(zz * pw + k * n, n), n)]

    def outward(m, d, k):
        at = part_blk(m, z + d * toward, k)
        return remote(at, at, z_s.at[1], z_sem(m, d if k == 0 else 1 + d + 3 * k), outer)

    def came(m, slot):
        zz = zo if slot == 3 else z + (slot + 1) * toward
        return remote(blk(m, zz), blk(m, zz), z_s.at[0], z_sem(m, slot), inner)

    def came_part(m, slot, k):
        at = part_blk(m, z + (slot + 1) * toward, k)
        return remote(at, at, z_s.at[0], z_sem(m, slot if k == 0 else 1 + slot + 3 * k), inner)

    def piece_out(m, r):
        to_inner(m, r).start()

        @on_mid
        def _():
            to_outer(m, r).start()

    def own_now(m):
        for r in (1, 2, 3):
            p1_in(m, r).wait_recv()
            piece_out(m, r)

    def own_inner(m):
        p1_whole(m).wait_recv()
        to_inner(m).start()

    def own_outer(m):
        @on_mid
        def _():
            for k in range(cuts(m)):
                outward(m, 0, k).start()

    def pass_in(m):
        @on_mid
        def _():
            came(m, 3).wait_recv()
            on_inner(m).start()

    def pass_out(m, d):
        @on_mid
        def _():
            came(m, d - 1).wait_recv()
            for k in range(cuts(m)):
                outward(m, d, k).start()

    def need(f, c):
        if c >= PARTS:
            @on_end
            def _():
                came_part(3 * f + 2, c // PARTS - 1, c % PARTS).wait_recv()

    def drain(sem, ref):
        remote(ref, ref, sem, sem, sibling).wait_send()

    bufs = (normed1, normed2)

    def piece(tt, h):
        return pl.ds(pl.multiple_of(tt * half + h * quarter, 16), quarter)

    def ag(f, r, h):
        at = piece(t, h)
        return remote(bufs[f].at[0, at, :], bufs[f].at[r, at, :], ag_s.at[0], ag_r.at[r - 1, h], to_peer[r])

    def ag_on(f, h):
        at = piece(t, h)
        return remote(bufs[f].at[2 - h, at, :], bufs[f].at[3, at, :], ag_s.at[0], ag_r.at[2, h], to_peer[1 + h])

    def relay(f, r, h, tt):
        at = bufs[f].at[r, piece(tt, h), :]
        return remote(at, at, rel_s.at[0], rel_r.at[r], sibling)

    def ag_first(f):
        for r, h in ((2, 0), (1, 1)):
            ag(f, r, h).wait_recv()
            ag_on(f, h).start()
            relay(f, r, h, t).start()

    def ag_second(f):
        for r, h in ((2, 1), (1, 0)):
            ag(f, r, h).wait_recv()
            relay(f, r, h, t).start()

    def ag_far(f):
        for h in range(2):
            ag_on(f, h).wait_recv()
            relay(f, 3, h, t).start()

    zs = (z, zi, jnp.where(mid == 1, zo, z + 2 * toward), jnp.where(mid == 1, z + 2 * toward, z + 3 * toward))
    cwid = pw // PARTS
    chunks = LINE * PARTS
    lanes = [pl.ds(pl.multiple_of(zz * pw + k * cwid, cwid), cwid) for zz in zs for k in range(PARTS)]
    lanes_a = pl.ds(pl.multiple_of((1 - low) * pw, pw), 3 * pw)
    lanes_b = pl.ds(pl.multiple_of(low * 3 * pw, pw), pw)
    first, second = pl.ds(0, quarter), pl.ds(quarter, quarter)

    def to_sibling(f, c, r):
        return remote(prod.at[r, other, lanes[c]], sib.at[r, :, lanes[c]], sib_s.at[0], sib_r.at[c % 2, r], sibling)

    def rs(f, c, kind):
        at = lanes[c]
        src, dst, r = (
            (comb.at[2, first, at], diag.at[0, :, at], 1),
            (comb.at[2, second, at], diag.at[1, :, at], 2),
            (comb.at[0, first, at], rsr.at[0, first, at], 1),
            (comb.at[0, second, at], rsr.at[0, second, at], 1),
            (comb.at[1, second, at], rsr.at[1, second, at], 2),
            (comb.at[1, first, at], rsr.at[1, first, at], 2),
        )[kind]
        return remote(src, dst, rs_s.at[0], rs_r.at[c, min(kind, 2)], to_peer[r])

    def product(f, k, r, at):
        dims = (((1,), (1,)), ((), ()))
        return lax.dot_general(bufs[f][r, :, at], w[3 * f + k, :, at], dims, preferred_element_type=F32)

    def slot_in(f, r):
        @pl.when(r > (0 if f == 0 else -1))
        def _():
            at = bufs[f].at[r, other, :]
            remote(at, at, rel_s.at[0], rel_r.at[r], sibling).wait_recv()

    def silu(g):
        return g / (1.0 + jnp.exp(-g))

    every = slice(None)

    def begin_hidden(f, lo, hi):
        @pl.loop(lo, hi)
        def _(r):
            slot_in(f, r)
            acc_g[r] = silu(product(f, 0, r, every))
            acc_u[r] = product(f, 1, r, lanes_a)

    def end_hidden(f):
        @pl.loop(0, PLANE)
        def _(r):
            u = acc_u[r] + product(f, 1, r, lanes_b)
            hidden[r] = (acc_g[r] * u).astype(BF16)

    def whole_hidden(f, lo, hi):
        @pl.loop(lo, hi)
        def _(r):
            slot_in(f, r)
            g = silu(product(f, 0, r, every))
            hidden[r] = (g * product(f, 1, r, every)).astype(BF16)

    def all_came(*pairs):
        @on_end
        def _():
            for m, slot in pairs:
                came(m, slot).wait_recv()

    def down(f, c):
        at = lanes[c]

        @pl.loop(0, PLANE)
        def _(k):
            r = PLANE - 1 - k
            prod[r, :, at] = jnp.dot(hidden[r], w[3 * f + 2, :, at], preferred_element_type=F32).astype(BF16)
            to_sibling(f, c, r).start()

        for r, kinds in ((3, (0, 1)), (2, (4,)), (1, (2,))):
            to_sibling(f, c, r).wait_recv()

            @pl.loop(0, half // (2 * step))
            def _(i):
                some = pl.ds(pl.multiple_of(i * 2 * step, step), 2 * step)
                full = pl.ds(pl.multiple_of(t * half + i * 2 * step, step), 2 * step)
                comb[r - 1, some, at] = (prod[r, full, at].astype(F32) + sib[r, some, at].astype(F32)).astype(BF16)

            for kind in kinds:
                rs(f, c, kind).start()
        to_sibling(f, c, 0).wait_recv()

    def finish(f, c):
        at = lanes[c]
        rs(f, c, 0).wait_recv()
        comb[1, first, at] = (comb[1, first, at].astype(F32) + diag[0, :, at].astype(F32)).astype(BF16)
        rs(f, c, 5).start()
        rs(f, c, 1).wait_recv()
        comb[0, second, at] = (comb[0, second, at].astype(F32) + diag[1, :, at].astype(F32)).astype(BF16)
        rs(f, c, 3).start()

    def reduced(rows_at, full, at):
        total = prod[0, full, at].astype(F32) + sib[0, rows_at, at].astype(F32)
        return total + rsr[0, rows_at, at].astype(F32) + rsr[1, rows_at, at].astype(F32)

    def out_across(c):
        at = lanes[c]
        return remote(here.at[:, at], fin.at[:, at], fin_s.at[0], fin_r.at[c], sibling)

    def out_store(c, k):
        at = lanes[c]
        return pltpu.make_async_copy((here, fin)[k].at[:, at], out_h.at[(mine, other)[k], at], store.at[0])

    def store_other(c):
        out_across(c).wait_recv()
        out_store(c, 1).start()

    def land(f, c):
        at = lanes[c]
        remote(rsr.at[:, :, at], rsr.at[:, :, at], rs_s.at[0], rs_r.at[c, 2], sibling).wait_recv()

        @pl.loop(0, half // (2 * step))
        def _(i):
            some = pl.ds(pl.multiple_of(i * 2 * step, step), 2 * step)
            full = pl.ds(pl.multiple_of(t * half + i * 2 * step, step), 2 * step)
            if f == 0:
                value = tokens[full, at].astype(F32) + merged[full, at].astype(F32) + 0.5 * reduced(some, full, at)
                middle[some, at] = value
                squares = value * value
                sums = sum(squares[:, k * 128:(k + 1) * 128] for k in range(cwid // 128))
                ssq[some, :] = sums if c == 0 else ssq[some, :] + sums
            else:
                here[some, at] = (middle[some, at] + 0.5 * reduced(some, full, at)).astype(BF16)

        if f == 1:
            out_across(c).start()
            out_store(c, 0).start()

    def norm_first(start, count):
        @pl.loop(0, count // step)
        def _(i):
            at = pl.ds(pl.multiple_of(start + i * step, step), step)
            normed1[0, at, :] = norm_rows(tokens[at, :].astype(F32), gain1[...]).astype(BF16)

    turn(0)
    place(0)
    pl.semaphore_wait(barrier, len(targets) + mid)
    start_p1(0)
    piece_out(0, 0)
    turn(1)
    start_p1(1)
    place(1)
    piece_out(1, 0)

    load_tokens.wait()
    load_gain1.wait()
    norm_first(t * half, half)
    for r, h in ((2, 0), (1, 1), (2, 1), (1, 0)):
        ag(0, r, h).start()
    loading(2).wait()
    start_p1(2)
    place(2)
    own_now(0)
    norm_first((1 - t) * half, half)
    own_now(1)
    turn(3)
    turn(4)
    pass_in(0)
    pass_out(0, 1)
    pass_in(1)
    pass_out(1, 1)
    ag_first(0)
    loading(5).wait()
    for m in (3, 4, 5):
        start_p1(m)
        place(m)
    pass_out(0, 2)
    ag_second(0)
    own_inner(2)
    begin_hidden(0, 0, 3 * mid)
    pass_out(1, 2)
    own_outer(2)
    ag_far(0)

    all_came((0, 0), (0, 1), (0, 2), (1, 0), (1, 1))
    begin_hidden(0, 3 * mid, PLANE)

    @on_end
    def _():
        for m in (3, 4, 5):
            own_inner(m)

    all_came((1, 2))
    end_hidden(0)
    pass_in(2)
    pass_out(2, 1)

    @on_mid
    def _():
        own_inner(3)

    down(0, 0)
    down(0, 1)
    finish(0, 0)
    for c in range(2, chunks):
        need(0, c)
        down(0, c)
        finish(0, c - 1)
        if c == 3:
            load_merged.wait()
            load_gain2.wait()
        if c >= 3:
            land(0, c - 3)
        if c == 4:
            pass_out(2, 2)
            own_outer(3)
        if c == 5:
            pass_in(3)
            pass_out(3, 1)

            @on_mid
            def _():
                own_inner(4)

    land(0, 5)
    finish(0, 7)
    pass_in(4)

    @on_mid
    def _():
        own_inner(5)

    land(0, 6)
    land(0, 7)
    drain(ag_s.at[0], normed1.at[pl.ds(0, 3), pl.ds(0, half), :])
    drain(rel_s.at[0], normed1.at[pl.ds(0, 3), pl.ds(0, half), :])

    @pl.loop(0, half // step)
    def _(i):
        at = pl.ds(pl.multiple_of(i * step, step), step)
        full = pl.ds(pl.multiple_of(t * half + i * step, step), step)
        scale = lax.rsqrt(jnp.sum(ssq[at, :], axis=-1, keepdims=True) / width + EPS)
        normed2[0, full, :] = (middle[at, :] * scale * gain2[...]).astype(BF16)

    for r, h in ((2, 0), (1, 1), (2, 1), (1, 0)):
        ag(1, r, h).start()
    for h in range(2):
        relay(1, 0, h, t).start()
    pass_out(3, 2)
    own_outer(4)
    pass_in(5)
    pass_out(4, 1)
    ag_first(1)
    pass_out(4, 2)
    own_outer(5)
    ag_second(1)
    pass_out(5, 1)

    @on_mid
    def _():
        whole_hidden(1, 0, 3)

    all_came((3, 0), (3, 1), (3, 2), (4, 0), (4, 1))
    begin_hidden(1, 0, 3 - 3 * mid)
    ag_far(1)
    drain(sib_s.at[0], sib)
    drain(rs_s.at[0], comb)

    @on_mid
    def _():
        whole_hidden(1, 3, 4)

    pass_out(5, 2)

    @on_end
    def _():
        begin_hidden(1, 3, 4)
        came(4, 2).wait_recv()
        end_hidden(1)

    down(1, 0)
    down(1, 1)
    finish(1, 0)
    for c in range(2, chunks):
        need(1, c)
        down(1, c)
        finish(1, c - 1)
        if 3 <= c < chunks - 1:
            land(1, c - 3)
    land(1, chunks - 4)
    land(1, chunks - 3)
    for c in range(chunks - 4):
        store_other(c)
    finish(1, chunks - 1)
    land(1, chunks - 2)
    land(1, chunks - 1)

    for c in range(chunks - 4, chunks):
        store_other(c)
    drain(p1_s.at[0], w.at[:, :, pl.ds(0, (PLANE - 1) * ds)])

    @on_mid
    def _():
        drain(z_s.at[0], w.at[:, :, pl.ds(0, 2 * pw)])
        drain(z_s.at[1], w.at[:, :, pl.ds(0, 3 * pw)])

    @on_end
    def _():
        drain(z_s.at[0], w.at[:, :, pl.ds(0, pw)])

    drain(ag_s.at[0], normed2.at[pl.ds(0, 3), pl.ds(0, half), :])
    drain(rel_s.at[0], normed2.at[:, pl.ds(0, half), :])
    drain(sib_s.at[0], sib)
    drain(rs_s.at[0], comb)
    drain(fin_s.at[0], here)
    pltpu.make_async_copy(tokens, tokens, store.at[0]).wait()


def plane_shards(tokens, merged, gain1, g1, u1, d1, gain2, g2, u2, d2):
    rows, width = tokens.shape
    half = rows // 2
    hid, ds = d1.shape
    q = hid // PLANE
    chunks = LINE * PARTS
    far = pl.BlockSpec(memory_space=pl.ANY)
    dma = lambda *s: pltpu.SemaphoreType.DMA(s)
    return pl.pallas_call(
        kernel,
        out_shape=pltpu.VMEM((rows, width), BF16),
        in_specs=[far] * 10,
        out_specs=far,
        scratch_shapes=[
            pltpu.VMEM((4, ds, hid), BF16),
            pltpu.VMEM((4, hid, ds), BF16),
            pltpu.VMEM((2, hid, ds), BF16),
            pltpu.VMEM((rows, width), BF16),
            pltpu.VMEM((rows, width), BF16),
            pltpu.VMEM((1, width), F32),
            pltpu.VMEM((1, width), F32),
            pltpu.VMEM((half, width), BF16),
            pltpu.VMEM((half, width), BF16),
            pltpu.VMEM((6, q, width), BF16),
            pltpu.VMEM((PLANE, rows, width), BF16),
            pltpu.VMEM((PLANE, rows, width), BF16),
            pltpu.VMEM((PLANE, rows, q), F32),
            pltpu.VMEM((PLANE, rows, q), F32),
            pltpu.VMEM((PLANE, rows, q), BF16),
            pltpu.VMEM((PLANE, rows, width), BF16),
            pltpu.VMEM((PLANE, half, width), BF16),
            pltpu.VMEM((PLANE - 1, half, width), BF16),
            pltpu.VMEM((2, half // 2, width), BF16),
            pltpu.VMEM((2, half, width), BF16),
            pltpu.VMEM((half, width), F32),
            pltpu.VMEM((half, 128), F32),
            dma(10), dma(1), dma(10), dma(2), dma(24 + 2 * (3 * PARTS - 3)),
            dma(1), dma(3, 2), dma(1), dma(PLANE),
            dma(1), dma(2, PLANE), dma(1), dma(chunks, 3),
            dma(1), dma(chunks), dma(1),
        ],
        compiler_params=pltpu.CompilerParams(
            collective_id=0, has_side_effects=True, vmem_limit_bytes=60 * 2**20
        ),
    )(tokens, merged, gain1[None], gain2[None], g1, u1, d1, g2, u2, d2)


def shards(n_fs, n_tp, *args):
    rows, width = args[0].shape
    hid, cols = args[5].shape
    fits = n_fs == PLANE * LINE and n_tp == 2 and cols % 128 == 0 and width % (128 * LINE * PARTS) == 0
    fits = fits and hid % (32 * PLANE) == 0 and rows % 64 == 0
    return plane_shards(*args) if fits else gathered_shards(*args)


def solution(mesh):
    return jax.shard_map(
        functools.partial(shards, mesh.shape["fs"], mesh.shape["tp"]),
        mesh=mesh,
        in_specs=(
            P("fs", None),
            P("fs", None),
            P(),
            P("fs", "tp"),
            P("fs", "tp"),
            P("tp", "fs"),
            P(),
            P("fs", "tp"),
            P("fs", "tp"),
            P("tp", "fs"),
        ),
        out_specs=P("fs", None),
        check_vma=False,
    )
```

time: 168 us -> 160 us (0.952)
  Pallas kernels: 164 us -> 159 us
    pallas_call x1, Pallas kernels: 164 us -> 159 us  [plane_shards(): pl.pallas_call(kernel, out_shape=pltpu.VMEM((rows, width), BF16), in_spec...]
where the time goes in v3:
time: 160 us
  Pallas kernels  159 us (99%)
    pallas_call x1, Pallas kernels, plane_shards(): pl.pallas_call(kernel, out_shape=pltpu.VMEM((rows, width), BF16), in_spec...  159 us

profile of v3, /device:TPU:0, one launch (start us, length us, event | category | flops | bytes accessed | tf_op | source)
XLA Modules:
  0.0 159.9 jit_solution(12398147530257914254)
XLA Ops:
  0.0 158.8 %shard_map.100 = bf16[384,2048]{1,0:T(8,128)(2,1)S(1)} custom-call(bf16[384,2048]{1,0:T(8,128)(2,1)} %tokens_h.1, bf16[384,2048]{1,0:T(8,128)(2,1)} %merged_h.1, f32[1,2048]{1,0:T(1,128)} %bitcast.2, f32[1,2048]{1,0:T(1,128)} %bitcast.3, bf16[128,1408]{1,0:T(8,128)(2,1)} %wa.1, bf16[128,1408]{1,0:T(8,128)(2,1)} %wb.1, bf16[1408,128]{1,0:T(8,128)(2,1)} %wc.1, ...), custom_call_target="tpu_custom_call" | custom-call | tf_op jit(solution)/shard_map/pallas_call | solution.py:589
  158.8 1.1 copy.12

commit v4 on v3

--- a/solution.py
+++ b/solution.py
@@ -105,7 +105,7 @@
         loading(m).start()
     load_tokens.start()
     load_gain1.start()
-    for m in (2, 3, 4, 5):
+    for m in (3, 4, 2, 5):
         loading(m).start()
     load_merged.start()
     load_gain2.start()
@@ -181,6 +181,8 @@
         at = part_blk(m, z + d * toward, k)
         return remote(at, at, z_s.at[1], z_sem(m, d if k == 0 else 1 + d + 3 * k), outer)
 
+    early = (0, 1, 3, 4)
+
     def came(m, slot):
         zz = zo if slot == 3 else z + (slot + 1) * toward
         return remote(blk(m, zz), blk(m, zz), z_s.at[0], z_sem(m, slot), inner)
@@ -203,13 +205,21 @@
 
     def own_inner(m):
         p1_whole(m).wait_recv()
-        to_inner(m).start()
+        if m in early:
+            for r in (1, 2, 3):
+                to_inner(m, r).start()
+        else:
+            to_inner(m).start()
 
     def own_outer(m):
         @on_mid
         def _():
-            for k in range(cuts(m)):
-                outward(m, 0, k).start()
+            if m in early:
+                for r in (1, 2, 3):
+                    to_outer(m, r).start()
+            else:
+                for k in range(cuts(m)):
+                    outward(m, 0, k).start()
 
     def pass_in(m):
         @on_mid
@@ -304,6 +314,17 @@
 
     every = slice(None)
 
+    def gate_slots(f, lo, hi):
+        @pl.loop(lo, hi)
+        def _(r):
+            slot_in(f, r)
+            acc_g[r] = silu(product(f, 0, r, every))
+
+    def up_slots(f, lo, hi):
+        @pl.loop(lo, hi)
+        def _(r):
+            acc_u[r] = product(f, 1, r, lanes_a)
+
     def begin_hidden(f, lo, hi):
         @pl.loop(lo, hi)
         def _(r):
@@ -311,11 +332,17 @@
             acc_g[r] = silu(product(f, 0, r, every))
             acc_u[r] = product(f, 1, r, lanes_a)
 
+    def first_product(f, r):
+        prod[r, :, lanes[0]] = jnp.dot(hidden[r], w[3 * f + 2, :, lanes[0]], preferred_element_type=F32).astype(BF16)
+        to_sibling(f, 0, r).start()
+
     def end_hidden(f):
         @pl.loop(0, PLANE)
-        def _(r):
+        def _(k):
+            r = PLANE - 1 - k
             u = acc_u[r] + product(f, 1, r, lanes_b)
             hidden[r] = (acc_g[r] * u).astype(BF16)
+            first_product(f, r)
 
     def whole_hidden(f, lo, hi):
         @pl.loop(lo, hi)
@@ -323,6 +350,7 @@
             slot_in(f, r)
             g = silu(product(f, 0, r, every))
             hidden[r] = (g * product(f, 1, r, every)).astype(BF16)
+            first_product(f, r)
 
     def all_came(*pairs):
         @on_end
@@ -333,7 +361,7 @@
     def down(f, c):
         at = lanes[c]
 
-        @pl.loop(0, PLANE)
+        @pl.loop(0, PLANE if c else 0)
         def _(k):
             r = PLANE - 1 - k
             prod[r, :, at] = jnp.dot(hidden[r], w[3 * f + 2, :, at], preferred_element_type=F32).astype(BF16)
@@ -413,6 +441,10 @@
     start_p1(1)
     place(1)
     piece_out(1, 0)
+    for m in (3, 4):
+        turn(m)
+        place(m)
+        piece_out(m, 0)
 
     load_tokens.wait()
     load_gain1.wait()
@@ -425,17 +457,15 @@
     own_now(0)
     norm_first((1 - t) * half, half)
     own_now(1)
-    turn(3)
-    turn(4)
     pass_in(0)
     pass_out(0, 1)
     pass_in(1)
     pass_out(1, 1)
     ag_first(0)
     loading(5).wait()
+    place(5)
     for m in (3, 4, 5):
         start_p1(m)
-        place(m)
     pass_out(0, 2)
     ag_second(0)
     own_inner(2)
@@ -518,16 +548,18 @@
     ag_second(1)
     pass_out(5, 1)
 
-    @on_mid
-    def _():
-        whole_hidden(1, 0, 3)
-
-    all_came((3, 0), (3, 1), (3, 2), (4, 0), (4, 1))
-    begin_hidden(1, 0, 3 - 3 * mid)
-    ag_far(1)
     drain(sib_s.at[0], sib)
     drain(rs_s.at[0], comb)
 
+    @on_mid
+    def _():
+        whole_hidden(1, 0, 3)
+
+    all_came((3, 0), (3, 1), (3, 2))
+    gate_slots(1, 0, 3 - 3 * mid)
+    all_came((4, 0), (4, 1))
+    up_slots(1, 0, 3 - 3 * mid)
+    ag_far(1)
     @on_mid
     def _():
         whole_hidden(1, 3, 4)

time: 160 us -> 157 us (0.981)
  Pallas kernels: 159 us -> 155 us
    pallas_call x1, Pallas kernels: 159 us -> 155 us  [plane_shards(): pl.pallas_call(kernel, out_shape=pltpu.VMEM((rows, width), BF16), in_spec...]
where the time goes in v4:
time: 157 us
  Pallas kernels  155 us (99%)
    pallas_call x1, Pallas kernels, plane_shards(): pl.pallas_call(kernel, out_shape=pltpu.VMEM((rows, width), BF16), in_spec...  155 us

profile of v4, /device:TPU:0, one launch (start us, length us, event | category | flops | bytes accessed | tf_op | source)
XLA Modules:
  0.0 156.5 jit_solution(5107277557303180017)
XLA Ops:
  0.0 155.4 %shard_map.100 = bf16[384,2048]{1,0:T(8,128)(2,1)S(1)} custom-call(bf16[384,2048]{1,0:T(8,128)(2,1)} %tokens_h.1, bf16[384,2048]{1,0:T(8,128)(2,1)} %merged_h.1, f32[1,2048]{1,0:T(1,128)} %bitcast.2, f32[1,2048]{1,0:T(1,128)} %bitcast.3, bf16[128,1408]{1,0:T(8,128)(2,1)} %wa.1, bf16[128,1408]{1,0:T(8,128)(2,1)} %wb.1, bf16[1408,128]{1,0:T(8,128)(2,1)} %wc.1, ...), custom_call_target="tpu_custom_call" | custom-call | tf_op jit(solution)/shard_map/pallas_call | solution.py:621
  155.4 1.1 copy.12

commit v5 on v4

--- a/solution.py
+++ b/solution.py
@@ -12,7 +12,6 @@
 F32 = jnp.float32
 PLANE = 4
 LINE = 4
-PARTS = 2
 
 
 def norm_rows(values, gain):
@@ -78,6 +77,9 @@
     def on_end(f):
         pl.when(mid == 0)(f)
 
+    HALVES = ((0, pw // 2), (pw // 2, pw // 2))
+    LAST = ((0, pw // 2), (pw // 2, pw // 4), (3 * pw // 4, pw // 4))
+
     def remote(src, dst, s, r, to):
         return pltpu.make_async_remote_copy(
             src_ref=src, dst_ref=dst, send_sem=s, recv_sem=r,
@@ -154,10 +156,8 @@
         return w.at[m, :, pl.ds(pl.multiple_of(zz * pw, pw), pw)]
 
     first_slot = 3 * (1 - mid)
-    wide = 1 + 3 * PARTS
-
     def z_sem(m, slot):
-        return z_r.at[4 * m + (m // 3) * (wide - 4) + slot]
+        return z_r.at[(0, 4, 9, 16, 20, 25)[m] + slot]
 
     def to_inner(m, r=None):
         at = blk(m, z) if r is None else w.at[m, :, lanes_of(z, peers[r])]
@@ -170,16 +170,19 @@
     def on_inner(m):
         return remote(blk(m, zo), blk(m, zo), z_s.at[0], z_sem(m, 1), inner)
 
-    def cuts(m):
-        return PARTS if m % 3 == 2 else 1
-
-    def part_blk(m, zz, k):
-        n = pw // cuts(m)
-        return w.at[m, :, pl.ds(pl.multiple_of(zz * pw + k * n, n), n)]
+    def cuts(m, d):
+        if m % 3 == 1 and d == 2:
+            return HALVES
+        if m % 3 < 2:
+            return ((0, pw),)
+        if m == 5 and d == 2:
+            return LAST
+        return HALVES
 
     def outward(m, d, k):
-        at = part_blk(m, z + d * toward, k)
-        return remote(at, at, z_s.at[1], z_sem(m, d if k == 0 else 1 + d + 3 * k), outer)
+        lo, n = cuts(m, d)[k]
+        at = w.at[m, :, pl.ds(pl.multiple_of((z + d * toward) * pw + lo, 128), n)]
+        return remote(at, at, z_s.at[1], z_sem(m, (d, 4 + d if m % 3 == 2 else 4, 7)[k]), outer)
 
     early = (0, 1, 3, 4)
 
@@ -188,8 +191,9 @@
         return remote(blk(m, zz), blk(m, zz), z_s.at[0], z_sem(m, slot), inner)
 
     def came_part(m, slot, k):
-        at = part_blk(m, z + (slot + 1) * toward, k)
-        return remote(at, at, z_s.at[0], z_sem(m, slot if k == 0 else 1 + slot + 3 * k), inner)
+        lo, n = cuts(m, slot)[k]
+        at = w.at[m, :, pl.ds(pl.multiple_of((z + (slot + 1) * toward) * pw + lo, 128), n)]
+        return remote(at, at, z_s.at[0], z_sem(m, (slot, 4 + slot if m % 3 == 2 else 4, 7)[k]), inner)
 
     def piece_out(m, r):
         to_inner(m, r).start()
@@ -206,8 +210,14 @@
     def own_inner(m):
         p1_whole(m).wait_recv()
         if m in early:
-            for r in (1, 2, 3):
-                to_inner(m, r).start()
+            @pl.when(t == 0)
+            def _():
+                for r in (1, 2, 3):
+                    to_inner(m, r).start()
+
+            @pl.when(t == 1)
+            def _():
+                to_inner(m).start()
         else:
             to_inner(m).start()
 
@@ -215,10 +225,16 @@
         @on_mid
         def _():
             if m in early:
-                for r in (1, 2, 3):
-                    to_outer(m, r).start()
+                @pl.when(t == 0)
+                def _():
+                    for r in (1, 2, 3):
+                        to_outer(m, r).start()
+
+                @pl.when(t == 1)
+                def _():
+                    outward(m, 0, 0).start()
             else:
-                for k in range(cuts(m)):
+                for k in range(len(cuts(m, 0))):
                     outward(m, 0, k).start()
 
     def pass_in(m):
@@ -231,14 +247,15 @@
         @on_mid
         def _():
             came(m, d - 1).wait_recv()
-            for k in range(cuts(m)):
+            for k in range(len(cuts(m, d))):
                 outward(m, d, k).start()
 
     def need(f, c):
-        if c >= PARTS:
+        block, k = table[f][c]
+        if block:
             @on_end
             def _():
-                came_part(3 * f + 2, c // PARTS - 1, c % PARTS).wait_recv()
+                came_part(3 * f + 2, block - 1, k).wait_recv()
 
     def drain(sem, ref):
         remote(ref, ref, sem, sem, sibling).wait_send()
@@ -277,18 +294,21 @@
             relay(f, 3, h, t).start()
 
     zs = (z, zi, jnp.where(mid == 1, zo, z + 2 * toward), jnp.where(mid == 1, z + 2 * toward, z + 3 * toward))
-    cwid = pw // PARTS
-    chunks = LINE * PARTS
-    lanes = [pl.ds(pl.multiple_of(zz * pw + k * cwid, cwid), cwid) for zz in zs for k in range(PARTS)]
+    table = [[(b, k) for b in range(LINE) for k in range(len(cuts(3 * f + 2, b - 1)))] for f in range(2)]
+    sizes = [[cuts(3 * f + 2, b - 1)[k] for b, k in table[f]] for f in range(2)]
+    lanes = [
+        [pl.ds(pl.multiple_of(zs[b] * pw + lo, 128), n) for (b, k), (lo, n) in zip(table[f], sizes[f])]
+        for f in range(2)
+    ]
     lanes_a = pl.ds(pl.multiple_of((1 - low) * pw, pw), 3 * pw)
-    lanes_b = pl.ds(pl.multiple_of(low * 3 * pw, pw), pw)
+    lanes_b = [pl.ds(pl.multiple_of(low * 3 * pw + lo, 128), n) for lo, n in HALVES]
     first, second = pl.ds(0, quarter), pl.ds(quarter, quarter)
 
     def to_sibling(f, c, r):
-        return remote(prod.at[r, other, lanes[c]], sib.at[r, :, lanes[c]], sib_s.at[0], sib_r.at[c % 2, r], sibling)
+        return remote(prod.at[r, other, lanes[f][c]], sib.at[r, :, lanes[f][c]], sib_s.at[0], sib_r.at[c % 3, r], sibling)
 
     def rs(f, c, kind):
-        at = lanes[c]
+        at = lanes[f][c]
         src, dst, r = (
             (comb.at[2, first, at], diag.at[0, :, at], 1),
             (comb.at[2, second, at], diag.at[1, :, at], 2),
@@ -333,14 +353,19 @@
             acc_u[r] = product(f, 1, r, lanes_a)
 
     def first_product(f, r):
-        prod[r, :, lanes[0]] = jnp.dot(hidden[r], w[3 * f + 2, :, lanes[0]], preferred_element_type=F32).astype(BF16)
+        prod[r, :, lanes[f][0]] = jnp.dot(hidden[r], w[3 * f + 2, :, lanes[f][0]], preferred_element_type=F32).astype(BF16)
         to_sibling(f, 0, r).start()
+
+    def more_hidden(f):
+        @pl.loop(0, PLANE)
+        def _(r):
+            acc_u[r] = acc_u[r] + product(f, 1, r, lanes_b[0])
 
     def end_hidden(f):
         @pl.loop(0, PLANE)
         def _(k):
             r = PLANE - 1 - k
-            u = acc_u[r] + product(f, 1, r, lanes_b)
+            u = acc_u[r] + product(f, 1, r, lanes_b[1])
             hidden[r] = (acc_g[r] * u).astype(BF16)
             first_product(f, r)
 
@@ -358,30 +383,39 @@
             for m, slot in pairs:
                 came(m, slot).wait_recv()
 
-    def down(f, c):
-        at = lanes[c]
-
-        @pl.loop(0, PLANE if c else 0)
+    def combine(f, c, r):
+        at = lanes[f][c]
+        to_sibling(f, c, r).wait_recv()
+
+        @pl.loop(0, half // (2 * step))
+        def _(i):
+            some = pl.ds(pl.multiple_of(i * 2 * step, step), 2 * step)
+            full = pl.ds(pl.multiple_of(t * half + i * 2 * step, step), 2 * step)
+            comb[r - 1, some, at] = (prod[r, full, at].astype(F32) + sib[r, some, at].astype(F32)).astype(BF16)
+
+        for kind in (None, (2,), (4,), (0, 1))[r]:
+            rs(f, c, kind).start()
+
+    def combine_all(f, c):
+        for r in (3, 2, 1):
+            combine(f, c, r)
+        to_sibling(f, c, 0).wait_recv()
+
+    def produce(f, c):
+        at = lanes[f][c]
+
+        @pl.loop(0, PLANE)
         def _(k):
             r = PLANE - 1 - k
             prod[r, :, at] = jnp.dot(hidden[r], w[3 * f + 2, :, at], preferred_element_type=F32).astype(BF16)
             to_sibling(f, c, r).start()
 
-        for r, kinds in ((3, (0, 1)), (2, (4,)), (1, (2,))):
-            to_sibling(f, c, r).wait_recv()
-
-            @pl.loop(0, half // (2 * step))
-            def _(i):
-                some = pl.ds(pl.multiple_of(i * 2 * step, step), 2 * step)
-                full = pl.ds(pl.multiple_of(t * half + i * 2 * step, step), 2 * step)
-                comb[r - 1, some, at] = (prod[r, full, at].astype(F32) + sib[r, some, at].astype(F32)).astype(BF16)
-
-            for kind in kinds:
-                rs(f, c, kind).start()
-        to_sibling(f, c, 0).wait_recv()
+    def down(f, c):
+        produce(f, c)
+        combine_all(f, c)
 
     def finish(f, c):
-        at = lanes[c]
+        at = lanes[f][c]
         rs(f, c, 0).wait_recv()
         comb[1, first, at] = (comb[1, first, at].astype(F32) + diag[0, :, at].astype(F32)).astype(BF16)
         rs(f, c, 5).start()
@@ -394,11 +428,11 @@
         return total + rsr[0, rows_at, at].astype(F32) + rsr[1, rows_at, at].astype(F32)
 
     def out_across(c):
-        at = lanes[c]
+        at = lanes[1][c]
         return remote(here.at[:, at], fin.at[:, at], fin_s.at[0], fin_r.at[c], sibling)
 
     def out_store(c, k):
-        at = lanes[c]
+        at = lanes[1][c]
         return pltpu.make_async_copy((here, fin)[k].at[:, at], out_h.at[(mine, other)[k], at], store.at[0])
 
     def store_other(c):
@@ -406,7 +440,7 @@
         out_store(c, 1).start()
 
     def land(f, c):
-        at = lanes[c]
+        at = lanes[f][c]
         remote(rsr.at[:, :, at], rsr.at[:, :, at], rs_s.at[0], rs_r.at[c, 2], sibling).wait_recv()
 
         @pl.loop(0, half // (2 * step))
@@ -417,7 +451,7 @@
                 value = tokens[full, at].astype(F32) + merged[full, at].astype(F32) + 0.5 * reduced(some, full, at)
                 middle[some, at] = value
                 squares = value * value
-                sums = sum(squares[:, k * 128:(k + 1) * 128] for k in range(cwid // 128))
+                sums = sum(squares[:, k * 128:(k + 1) * 128] for k in range(sizes[f][c][1] // 128))
                 ssq[some, :] = sums if c == 0 else ssq[some, :] + sums
             else:
                 here[some, at] = (middle[some, at] + 0.5 * reduced(some, full, at)).astype(BF16)
@@ -444,7 +478,11 @@
     for m in (3, 4):
         turn(m)
         place(m)
-        piece_out(m, 0)
+
+    @pl.when(t == 0)
+    def _():
+        for m in (3, 4):
+            piece_out(m, 0)
 
     load_tokens.wait()
     load_gain1.wait()
@@ -482,8 +520,18 @@
         for m in (3, 4, 5):
             own_inner(m)
 
-    all_came((1, 2))
+    @on_end
+    def _():
+        came_part(1, 2, 0).wait_recv()
+
+    more_hidden(0)
+
+    @on_end
+    def _():
+        came_part(1, 2, 1).wait_recv()
+
     end_hidden(0)
+    combine_all(0, 0)
     pass_in(2)
     pass_out(2, 1)
 
@@ -491,10 +539,9 @@
     def _():
         own_inner(3)
 
-    down(0, 0)
     down(0, 1)
     finish(0, 0)
-    for c in range(2, chunks):
+    for c in range(2, len(table[0])):
         need(0, c)
         down(0, c)
         finish(0, c - 1)
@@ -563,29 +610,42 @@
     @on_mid
     def _():
         whole_hidden(1, 3, 4)
+        combine_all(1, 0)
 
     pass_out(5, 2)
 
     @on_end
     def _():
         begin_hidden(1, 3, 4)
-        came(4, 2).wait_recv()
+        came_part(4, 2, 0).wait_recv()
+        more_hidden(1)
+        came_part(4, 2, 1).wait_recv()
         end_hidden(1)
-
-    down(1, 0)
+        combine_all(1, 0)
+
+    chunks = len(table[1])
     down(1, 1)
     finish(1, 0)
-    for c in range(2, chunks):
+    for c in range(2, chunks - 2):
         need(1, c)
         down(1, c)
         finish(1, c - 1)
-        if 3 <= c < chunks - 1:
+        if c >= 3:
             land(1, c - 3)
+    need(1, chunks - 2)
+    produce(1, chunks - 2)
+    need(1, chunks - 1)
+    produce(1, chunks - 1)
+    combine_all(1, chunks - 2)
+    combine_all(1, chunks - 1)
+    finish(1, chunks - 3)
+    finish(1, chunks - 2)
+    land(1, chunks - 5)
     land(1, chunks - 4)
-    land(1, chunks - 3)
     for c in range(chunks - 4):
         store_other(c)
     finish(1, chunks - 1)
+    land(1, chunks - 3)
     land(1, chunks - 2)
     land(1, chunks - 1)
 
@@ -615,7 +675,7 @@
     half = rows // 2
     hid, ds = d1.shape
     q = hid // PLANE
-    chunks = LINE * PARTS
+    chunks = 2 * LINE + 1
     far = pl.BlockSpec(memory_space=pl.ANY)
     dma = lambda *s: pltpu.SemaphoreType.DMA(s)
     return pl.pallas_call(
@@ -646,9 +706,9 @@
             pltpu.VMEM((2, half, width), BF16),
             pltpu.VMEM((half, width), F32),
             pltpu.VMEM((half, 128), F32),
-            dma(10), dma(1), dma(10), dma(2), dma(24 + 2 * (3 * PARTS - 3)),
+            dma(10), dma(1), dma(10), dma(2), dma(33),
             dma(1), dma(3, 2), dma(1), dma(PLANE),
-            dma(1), dma(2, PLANE), dma(1), dma(chunks, 3),
+            dma(1), dma(3, PLANE), dma(1), dma(chunks, 3),
             dma(1), dma(chunks), dma(1),
         ],
         compiler_params=pltpu.CompilerParams(
@@ -660,7 +720,7 @@
 def shards(n_fs, n_tp, *args):
     rows, width = args[0].shape
     hid, cols = args[5].shape
-    fits = n_fs == PLANE * LINE and n_tp == 2 and cols % 128 == 0 and width % (128 * LINE * PARTS) == 0
+    fits = n_fs == PLANE * LINE and n_tp == 2 and cols % 128 == 0 and width % (512 * LINE) == 0
     fits = fits and hid % (32 * PLANE) == 0 and rows % 64 == 0
     return plane_shards(*args) if fits else gathered_shards(*args)
 

time: 157 us -> 156 us (level)
  no operation moved by 1% of the time
where the time goes in v5:
time: 156 us
  Pallas kernels  155 us (99%)
    pallas_call x1, Pallas kernels, plane_shards(): pl.pallas_call(kernel, out_shape=pltpu.VMEM((rows, width), BF16), in_spec...  155 us

profile of v5, /device:TPU:0, one launch (start us, length us, event | category | flops | bytes accessed | tf_op | source)
XLA Modules:
  0.0 156.0 jit_solution(4777173577075582888)
XLA Ops:
  0.0 154.8 %shard_map.100 = bf16[384,2048]{1,0:T(8,128)(2,1)S(1)} custom-call(bf16[384,2048]{1,0:T(8,128)(2,1)} %tokens_h.1, bf16[384,2048]{1,0:T(8,128)(2,1)} %merged_h.1, f32[1,2048]{1,0:T(1,128)} %bitcast.2, f32[1,2048]{1,0:T(1,128)} %bitcast.3, bf16[128,1408]{1,0:T(8,128)(2,1)} %wa.1, bf16[128,1408]{1,0:T(8,128)(2,1)} %wb.1, bf16[1408,128]{1,0:T(8,128)(2,1)} %wc.1, ...), custom_call_target="tpu_custom_call" | custom-call | tf_op jit(solution)/shard_map/pallas_call | solution.py:681
  154.8 1.1 copy.12

commit v6 on v5

--- a/solution.py
+++ b/solution.py
@@ -155,9 +155,9 @@
     def blk(m, zz):
         return w.at[m, :, pl.ds(pl.multiple_of(zz * pw, pw), pw)]
 
-    first_slot = 3 * (1 - mid)
+    first_slot = 2 * (1 - mid)
     def z_sem(m, slot):
-        return z_r.at[(0, 4, 9, 16, 20, 25)[m] + slot]
+        return z_r.at[(0, 3, 7, 13, 16, 20)[m] + slot]
 
     def to_inner(m, r=None):
         at = blk(m, z) if r is None else w.at[m, :, lanes_of(z, peers[r])]
@@ -182,18 +182,18 @@
     def outward(m, d, k):
         lo, n = cuts(m, d)[k]
         at = w.at[m, :, pl.ds(pl.multiple_of((z + d * toward) * pw + lo, 128), n)]
-        return remote(at, at, z_s.at[1], z_sem(m, (d, 4 + d if m % 3 == 2 else 4, 7)[k]), outer)
+        return remote(at, at, z_s.at[1], z_sem(m, (d, 3 + d if m % 3 == 2 else 3, 6)[k]), outer)
 
     early = (0, 1, 3, 4)
 
     def came(m, slot):
         zz = zo if slot == 3 else z + (slot + 1) * toward
-        return remote(blk(m, zz), blk(m, zz), z_s.at[0], z_sem(m, slot), inner)
+        return remote(blk(m, zz), blk(m, zz), z_s.at[0], z_sem(m, min(slot, 2)), inner)
 
     def came_part(m, slot, k):
         lo, n = cuts(m, slot)[k]
         at = w.at[m, :, pl.ds(pl.multiple_of((z + (slot + 1) * toward) * pw + lo, 128), n)]
-        return remote(at, at, z_s.at[0], z_sem(m, (slot, 4 + slot if m % 3 == 2 else 4, 7)[k]), inner)
+        return remote(at, at, z_s.at[0], z_sem(m, (slot, 3 + slot if m % 3 == 2 else 3, 6)[k]), inner)
 
     def piece_out(m, r):
         to_inner(m, r).start()
@@ -706,7 +706,7 @@
             pltpu.VMEM((2, half, width), BF16),
             pltpu.VMEM((half, width), F32),
             pltpu.VMEM((half, 128), F32),
-            dma(10), dma(1), dma(10), dma(2), dma(33),
+            dma(10), dma(1), dma(10), dma(2), dma(27),
             dma(1), dma(3, 2), dma(1), dma(PLANE),
             dma(1), dma(3, PLANE), dma(1), dma(chunks, 3),
             dma(1), dma(chunks), dma(1),

time: 156 us -> 156 us (level)
  no operation moved by 1% of the time
where the time goes in v6:
time: 156 us
  Pallas kernels  155 us (99%)
    pallas_call x1, Pallas kernels, plane_shards(): pl.pallas_call(kernel, out_shape=pltpu.VMEM((rows, width), BF16), in_spec...  155 us

profile of v6, /device:TPU:0, one launch (start us, length us, event | category | flops | bytes accessed | tf_op | source)
XLA Modules:
  0.0 155.9 jit_solution(3455870837734197545)
XLA Ops:
  0.0 154.8 %shard_map.100 = bf16[384,2048]{1,0:T(8,128)(2,1)S(1)} custom-call(bf16[384,2048]{1,0:T(8,128)(2,1)} %tokens_h.1, bf16[384,2048]{1,0:T(8,128)(2,1)} %merged_h.1, f32[1,2048]{1,0:T(1,128)} %bitcast.2, f32[1,2048]{1,0:T(1,128)} %bitcast.3, bf16[128,1408]{1,0:T(8,128)(2,1)} %wa.1, bf16[128,1408]{1,0:T(8,128)(2,1)} %wb.1, bf16[1408,128]{1,0:T(8,128)(2,1)} %wc.1, ...), custom_call_target="tpu_custom_call" | custom-call | tf_op jit(solution)/shard_map/pallas_call | solution.py:681
  154.8 1.1 copy.12
